TPU v7x, 32 devices: a whole 2x2x4 slice. The times are simulated.
32 devices in a mesh: grp: 2 (over y), sp: 4 (over z), tp: 4 (over x, core).
Axes of the slice: x: 2, y: 2, z: 4, core: 2. Of those that a mesh axis runs over, the one named last changes fastest.
Arguments:
- recurrent_query: bfloat16 [2048, 1024], P(('grp', 'sp'), 'tp'), parts along dimension 0, may hold values from -6 to 6
- recurrent_forget_gate: bfloat16 [2048, 1024], P(('grp', 'sp'), 'tp'), parts along dimension 0, may hold values from -4.5 to 4.5
- recurrent_value: bfloat16 [2048, 1024], P(('grp', 'sp'), 'tp'), parts along dimension 0, may hold values from -6 to 6
- recurrent_gate_lower_bound: float32 [1024], P('tp'), may hold values from 1.5 to 14
- recurrent_added_decay: float32 [2048, 8], P(('grp', 'sp'), 'tp'), parts along dimension 0, may hold values from -0.51 to 0
- recurrent_norm_gain: float32 [128], replicated, may hold values from 0.1 to 1.9
- attention_query_first: bfloat16 [2048, 512], P(('grp', 'sp'), 'tp'), parts along dimension 0, may hold values from -20 to 20
- attention_key_first: bfloat16 [2048, 256], P(('grp', 'sp'), 'tp'), parts along dimension 0, may hold values from -20 to 20
- attention_query_second: bfloat16 [2048, 512], P(('grp', 'sp'), 'tp'), parts along dimension 0, may hold values from -20 to 20
- attention_key_second: bfloat16 [2048, 256], P(('grp', 'sp'), 'tp'), parts along dimension 0, may hold values from -20 to 20
- attention_value: bfloat16 [2048, 512], P(('grp', 'sp'), 'tp'), parts along dimension 0, may hold values from -6 to 6
- second_map_weight: float32 [8], P('tp'), may hold values from 0.3 to 0.8
- attention_norm_gain: float32 [128], replicated, may hold values from 0.1 to 1.9
- output_weight: bfloat16 [2, 1024, 2048], P(None, 'tp', 'sp'), may hold values from -0.125 to 0.125
Outputs:
- mixed: bfloat16 [2048, 2048], P(('grp', 'sp', 'tp')), parts along dimension 0
There are 2 independent parts, one for each index of `grp`. A program takes and returns all parts, laid end to end along the dimension named above; an argument that names none is the same for every part. Nothing has to cross between parts.
All inputs are finite; a program needn't handle non-finite values.
Results may differ from a plain program's by a relative error of at most 0.02.
Values may be sent and summed in bfloat16 or wider, within the bound.
No kernel may reach another device: no remote copies, remote signals or barrier semaphores. Data moves between devices by JAX's collectives and lax.ppermute only.
A program may use at most 64 MiB of HBM per device.

v0:
```python
import functools

import jax
import jax.numpy as jnp
from jax import lax
from jax.experimental import pallas as pl
from jax.experimental.pallas import tpu as pltpu
from jax.sharding import PartitionSpec as P

HG_DK = 128
HG_DV = 128
DA_HD = 64
BLK = 32


epsilon = 1e-06
highest = lax.Precision.HIGHEST
key_span = 512


def carried_in(array, axis, combine, identity):
    size, place = (lax.axis_size(axis), lax.axis_index(axis))
    everything = jax.tree.map(
        lambda part, kind: lax.all_gather(part.astype(kind), axis),
        array,
        (jnp.bfloat16, jnp.bfloat16),
    )
    start = jax.tree.map(
        lambda part, zero: jnp.broadcast_to(jnp.asarray(zero, part.dtype), part.shape),
        array,
        identity,
    )

    def hop(k, before):
        reached = k < place
        new = combine(
            before, jax.tree.map(lambda part, own: part[k].astype(own.dtype), everything, array)
        )
        return jax.tree.map(lambda a, b: jnp.where(reached, a, b), new, before)

    return lax.fori_loop(0, size, hop, start)


def head_norm(head_values, gain_vec):
    mean_square = jnp.mean(head_values * head_values, axis=-1, keepdims=True)
    return head_values * lax.rsqrt(mean_square + epsilon) * gain_vec


def decay_factors(gate_preactivation, lower_bound_logit, added_log_decay, number_of_heads):
    token_count = gate_preactivation.shape[0]
    floor_rate = jax.nn.sigmoid(-lower_bound_logit).reshape(number_of_heads, -1)
    state_inflow = floor_rate[None] * jax.nn.sigmoid(
        -gate_preactivation.astype(jnp.float32)
    ).reshape(token_count, number_of_heads, -1)
    decay_logarithm = jnp.log1p(-state_inflow) + added_log_decay[:, :, None]
    return (state_inflow, decay_logarithm)


def recurrence_blocks(queries, decay_logarithm, state_inflow, value_rows, block_len):
    token_count, number_of_heads, key_width = queries.shape
    block_count = token_count // block_len

    def to_blocks(source):
        return source.reshape(block_count, block_len, number_of_heads, source.shape[-1])

    causal = jnp.tril(jnp.ones((block_len, block_len), jnp.float32))[:, :, None, None]

    def block_step(carry_state, inputs):
        query_blk, decay_blk, inflow_blk, value_blk = inputs
        cumulative = jnp.cumsum(decay_blk, axis=0)
        relative = cumulative[:, None] - cumulative[None, :]
        decay_table = jnp.exp(jnp.minimum(relative, 0.0)) * causal
        scores = jnp.einsum(
            "thd,shd,tshd->hts", query_blk, inflow_blk, decay_table, precision=highest
        )
        block_out = jnp.einsum("hts,shv->thv", scores, value_blk, precision=highest)
        block_out = block_out + jnp.einsum(
            "thd,hdv->thv", query_blk * jnp.exp(cumulative), carry_state, precision=highest
        )
        last_log = cumulative[-1]
        new_state = jnp.exp(last_log)[:, :, None] * carry_state + jnp.einsum(
            "shd,shv->hdv",
            inflow_blk * jnp.exp(last_log[None] - cumulative),
            value_blk,
            precision=highest,
        )
        return (new_state, block_out)

    zero_state = jnp.zeros((number_of_heads, key_width, value_rows.shape[-1]), jnp.float32)
    final_state, outputs = lax.scan(
        block_step,
        zero_state,
        (
            to_blocks(queries),
            to_blocks(decay_logarithm),
            to_blocks(state_inflow),
            to_blocks(value_rows),
        ),
    )
    return (final_state, outputs.reshape(token_count, number_of_heads, -1))


def chain_pair(earlier, following):
    return (earlier[0] * following[0], following[0][:, :, None] * earlier[1] + following[1])


def recurrent_path_output(
    recurrent_query,
    recurrent_forget_gate,
    recurrent_value,
    recurrent_gate_lower_bound,
    recurrent_added_decay,
    recurrent_norm_gain,
):
    token_count = recurrent_query.shape[0]
    number_of_heads = recurrent_gate_lower_bound.shape[0] // HG_DK
    state_inflow, decay_logarithm = decay_factors(
        recurrent_forget_gate, recurrent_gate_lower_bound, recurrent_added_decay, number_of_heads
    )
    queries = recurrent_query.astype(jnp.float32).reshape(token_count, number_of_heads, HG_DK)
    value_rows = recurrent_value.astype(jnp.float32).reshape(token_count, number_of_heads, HG_DV)
    final_state, local_out = recurrence_blocks(
        queries, decay_logarithm, state_inflow, value_rows, BLK
    )
    running_log = jnp.cumsum(decay_logarithm, axis=0)
    through = jnp.exp(running_log[-1])
    incoming = carried_in(
        (through, final_state),
        "sp",
        chain_pair,
        (jnp.ones_like(through), jnp.zeros_like(final_state)),
    )
    carried = jnp.einsum(
        "thd,hdv->thv", queries * jnp.exp(running_log), incoming[1], precision=highest
    )
    return (
        head_norm(local_out + carried, recurrent_norm_gain)
        .astype(jnp.bfloat16)
        .reshape(token_count, -1)
    )


def attention_branch(
    attention_query_first,
    attention_key_first,
    attention_query_second,
    attention_key_second,
    attention_value,
    second_map_weight,
    attention_norm_gain,
):
    query_rows = attention_query_first.shape[0]
    key_heads = attention_key_first.shape[1] // DA_HD
    group_size = attention_query_first.shape[1] // DA_HD // key_heads
    score_scale = DA_HD ** (-0.5)
    offset = lax.axis_index("sp") * query_rows
    query_pos = offset + jnp.arange(query_rows)
    last_query = offset + query_rows - 1
    queries_one = attention_query_first.reshape(query_rows, key_heads, group_size, DA_HD)
    queries_two = attention_query_second.reshape(query_rows, key_heads, group_size, DA_HD)

    def map_update(running, queries, key_rows, value_rows, allowed):
        row_max, weight_mass, value_sum = running
        scores = (
            jnp.einsum("qkgd,skd->kgqs", queries, key_rows, preferred_element_type=jnp.float32)
            * score_scale
        )
        scores = jnp.where(allowed, scores, -1e30)
        new_max = jnp.maximum(row_max, jnp.max(scores, axis=-1))
        weights = jnp.where(allowed, jnp.exp(scores - new_max[..., None]), 0.0)
        shrink = jnp.exp(row_max - new_max)
        weight_mass = weight_mass * shrink + jnp.sum(weights, axis=-1)
        value_sum = value_sum * shrink[..., None] + jnp.einsum(
            "plew,wpd->pled",
            weights.astype(jnp.bfloat16),
            value_rows,
            preferred_element_type=jnp.float32,
        )
        return (new_max, weight_mass, value_sum)

    def key_block(running, block_one, block_two, block_values, first_row):
        span_rows = block_one.shape[0]
        key_pos = first_row + jnp.arange(span_rows)
        allowed = key_pos[None, :] <= query_pos[:, None]
        shaped_one = block_one.reshape(span_rows, key_heads, DA_HD)
        shaped_two = block_two.reshape(span_rows, key_heads, DA_HD)
        shaped_values = block_values.reshape(span_rows, key_heads, 2 * DA_HD)
        return (
            map_update(running[0], queries_one, shaped_one, shaped_values, allowed),
            map_update(running[1], queries_two, shaped_two, shaped_values, allowed),
        )

    def guarded_block(running, block_one, block_two, block_values, first_row):

        def compute(state_in):
            return key_block(state_in, block_one, block_two, block_values, first_row)

        def unchanged(state_in):
            return state_in

        result = lax.cond(first_row > last_query, unchanged, compute, running)
        return result

    start_max = jnp.full((key_heads, group_size, query_rows), -1e30, jnp.float32)
    zero_mass = jnp.zeros((key_heads, group_size, query_rows), jnp.float32)
    zero_sum = jnp.zeros((key_heads, group_size, query_rows, 2 * DA_HD), jnp.float32)
    fresh_state = (start_max, zero_mass, zero_sum)
    running = (fresh_state, fresh_state)
    shard_one = lax.all_gather(attention_key_first, "sp", axis=0, tiled=True)
    shard_two = lax.all_gather(attention_key_second, "sp", axis=0, tiled=True)
    shard_values = lax.all_gather(attention_value, "sp", axis=0, tiled=True)
    row_count = shard_one.shape[0]
    span_rows = min(row_count, key_span)
    full_count = row_count // span_rows

    def span_step(span_index, state_in):
        begin_row = span_index * span_rows
        return guarded_block(
            state_in,
            lax.dynamic_slice_in_dim(shard_one, begin_row, span_rows, 0),
            lax.dynamic_slice_in_dim(shard_two, begin_row, span_rows, 0),
            lax.dynamic_slice_in_dim(shard_values, begin_row, span_rows, 0),
            begin_row,
        )

    running = lax.fori_loop(0, full_count, span_step, running)
    first_map, second_map = running
    lambda_table = second_map_weight.reshape(key_heads, group_size)[:, :, None, None]
    combined = first_map[2] / first_map[1][..., None] - lambda_table * (
        second_map[2] / second_map[1][..., None]
    )
    combined = jnp.transpose(combined, (2, 0, 1, 3)).reshape(
        query_rows, key_heads * group_size, 2 * DA_HD
    )
    return head_norm(combined, attention_norm_gain).astype(jnp.bfloat16).reshape(query_rows, -1)


def general_shards(
    recurrent_query,
    recurrent_forget_gate,
    recurrent_value,
    recurrent_gate_lower_bound,
    recurrent_added_decay,
    recurrent_norm_gain,
    attention_query_first,
    attention_key_first,
    attention_query_second,
    attention_key_second,
    attention_value,
    second_map_weight,
    attention_norm_gain,
    output_weight,
):
    attended = attention_branch(
        attention_query_first,
        attention_key_first,
        attention_query_second,
        attention_key_second,
        attention_value,
        second_map_weight,
        attention_norm_gain,
    )
    recurrent_output = recurrent_path_output(
        recurrent_query,
        recurrent_forget_gate,
        recurrent_value,
        recurrent_gate_lower_bound,
        recurrent_added_decay,
        recurrent_norm_gain,
    )
    pieces = lax.all_gather(output_weight, "sp", axis=2, tiled=True)
    partial_terms = jnp.dot(
        recurrent_output, pieces[0], preferred_element_type=jnp.float32
    ) + jnp.dot(attended, pieces[1], preferred_element_type=jnp.float32)
    return lax.psum_scatter(
        partial_terms.astype(jnp.bfloat16), "tp", scatter_dimension=0, tiled=True
    )


f32 = jnp.float32
bf16 = jnp.bfloat16
SPARE_ROWS = 16


PARAMS = pltpu.CompilerParams(vmem_limit_bytes=16 * 1024 * 1024)


def dot_nt(a, b):
    return lax.dot_general(a, b, (((1,), (1,)), ((), ())), preferred_element_type=f32)


def dot_nn(a, b):
    return jnp.dot(a, b, preferred_element_type=f32)


def dot_tn(a, b):
    return lax.dot_general(a, b, (((0,), (0,)), ((), ())), preferred_element_type=f32)


def cost(flops, *arrays):
    moved = sum(a.size * a.dtype.itemsize for a in arrays)
    return pl.CostEstimate(flops=flops, bytes_accessed=moved, transcendentals=0)


def recurrence_kernel(
    query_ref, gate_ref, value_ref, bound_ref, added_ref, local_ref, faded_ref, state_ref
):
    token_count, width = query_ref.shape
    heads = width // HG_DK
    chunk = min(token_count, HG_DK)
    floor_rate = jax.nn.sigmoid(-bound_ref[...])
    inflow = floor_rate * jax.nn.sigmoid(-gate_ref[...].astype(f32))
    added = added_ref[...]
    wide = [jnp.broadcast_to(added[:, h : h + 1], (token_count, HG_DK)) for h in range(heads)]
    log_decay = jnp.log1p(-inflow) + jnp.concatenate(wide, axis=1)
    row = lax.broadcasted_iota(jnp.int32, (chunk, chunk), 0)
    column = lax.broadcasted_iota(jnp.int32, (chunk, chunk), 1)
    causal = row >= column
    lower = jnp.where(causal, 1.0, 0.0).astype(bf16)
    total = jnp.zeros((1, width), f32)
    states = [None] * heads
    for n in range(token_count // chunk):
        rows = slice(n * chunk, (n + 1) * chunk)
        steps = log_decay[rows]
        coarse = steps.astype(bf16)
        fine = (steps - coarse.astype(f32)).astype(bf16)
        summed = dot_nn(lower, coarse) + dot_nn(lower, fine)
        last = summed[chunk - 1 : chunk]
        middle = summed[chunk // 2 - 1 : chunk // 2]
        query = query_ref[rows, :].astype(f32)
        inflow_rows = inflow[rows]
        near_query = (query * jnp.exp(summed - middle)).astype(bf16)
        near_key = (inflow_rows * jnp.exp(middle - summed)).astype(bf16)
        tail_key = (inflow_rows * jnp.exp(last - summed)).astype(bf16)
        faded = (query * jnp.exp(summed + total)).astype(bf16)
        faded_ref[rows, :] = faded
        if n:
            base_query = (query * jnp.exp(summed)).astype(bf16)
        fade = jnp.exp(last)
        for h in range(heads):
            lanes = slice(h * HG_DK, (h + 1) * HG_DK)
            value = value_ref[rows, lanes]
            scores = dot_nt(near_query[:, lanes], near_key[:, lanes])
            scores = jnp.where(causal, scores, 0.0).astype(bf16)
            out = dot_nn(scores, value)
            grown = dot_tn(value, tail_key[:, lanes])
            if n:
                out = out + dot_nt(base_query[:, lanes], states[h].astype(bf16))
                grown = grown + states[h] * fade[:, lanes]
            states[h] = grown
            local_ref[rows, lanes] = out
        total = total + last
    through = jnp.exp(total)
    for h in range(heads):
        lanes = slice(h * HG_DK, (h + 1) * HG_DK)
        state_ref[h, :HG_DV, :] = states[h].astype(bf16)
        state_ref[h, HG_DV:, :] = jnp.broadcast_to(through[:, lanes], (SPARE_ROWS, HG_DK)).astype(
            bf16
        )


def local_recurrence(query, gate, value, bound, added):
    token_count, width = query.shape
    heads = width // HG_DK
    outs = (
        jax.ShapeDtypeStruct((token_count, width), f32),
        jax.ShapeDtypeStruct((token_count, width), bf16),
        jax.ShapeDtypeStruct((heads, HG_DV + SPARE_ROWS, HG_DK), bf16),
    )
    return pl.pallas_call(
        recurrence_kernel,
        out_shape=outs,
        name="recurrence",
        compiler_params=PARAMS,
        cost_estimate=cost(16 * token_count * width * HG_DK, query, gate, value, *outs),
    )(query, gate, value, bound.reshape(1, -1), added)


def normed(values, gain):
    mean_square = jnp.mean(values * values, axis=-1, keepdims=True)
    return (values * lax.rsqrt(mean_square + epsilon) * gain).astype(bf16)


def carry_kernel(distances, local_ref, faded_ref, gain_ref, *refs):
    state_refs, out_ref = refs[:distances], refs[distances]
    heads = local_ref.shape[1] // HG_DV
    for h in range(heads):
        lanes = slice(h * HG_DV, (h + 1) * HG_DV)
        incoming = jnp.zeros((HG_DV, HG_DK), f32)
        for ref in reversed(state_refs):
            through = ref[h, HG_DV : HG_DV + 1, :].astype(f32)
            incoming = ref[h, :HG_DV, :].astype(f32) + through * incoming
        mixed = local_ref[:, lanes] + dot_nt(faded_ref[:, lanes], incoming.astype(bf16))
        out_ref[:, lanes] = normed(mixed, gain_ref[...])


def merge_kernel(near_ref, far_ref, out_ref):
    for h in range(near_ref.shape[0]):
        through = near_ref[h, HG_DV : HG_DV + 1, :].astype(f32)
        merged = near_ref[h].astype(f32) + through * far_ref[h].astype(f32)
        fade = through * far_ref[h, HG_DV:, :].astype(f32)
        out_ref[h, :HG_DV, :] = merged[:HG_DV].astype(bf16)
        out_ref[h, HG_DV:, :] = fade.astype(bf16)


def merge_states(near, far):
    return pl.pallas_call(
        merge_kernel,
        out_shape=jax.ShapeDtypeStruct(near.shape, bf16),
        name="merge",
        compiler_params=PARAMS,
        cost_estimate=cost(3 * near.size, near, far),
    )(near, far)


def carry_in(local, faded, gain, states):
    out = jax.ShapeDtypeStruct(local.shape, bf16)
    return pl.pallas_call(
        functools.partial(carry_kernel, len(states)),
        out_shape=out,
        name="carry",
        compiler_params=PARAMS,
        cost_estimate=cost(4 * local.size * HG_DK, local, faded, *states),
    )(local, faded, gain.reshape(1, -1), *states)


def attention_kernel(distances, lambda_ref, one_ref, two_ref, gain_ref, own_ref, *refs):
    other_refs, out_ref = refs[:distances], refs[distances]
    token_count = one_ref.shape[0]
    place = lax.axis_index("sp")
    tile = min(token_count, 2 * DA_HD)
    lane = lax.broadcasted_iota(jnp.int32, (tile, 2 * DA_HD), 1)
    blocks = (own_ref, *other_refs)
    wide = 2 * DA_HD
    ones = jnp.ones((token_count, wide), bf16)
    valued = [jnp.concatenate([ref[:, wide : 2 * wide], ones], axis=1) for ref in blocks]
    for t in range(token_count // tile):
        rows = slice(t * tile, (t + 1) * tile)
        row = lax.broadcasted_iota(jnp.int32, (tile, token_count), 0) + t * tile
        column = lax.broadcasted_iota(jnp.int32, (tile, token_count), 1)
        causal = row >= column
        for head in range(2):
            maps = []
            for m, ref in enumerate((one_ref, two_ref)):
                query = ref[rows, :].astype(f32) * DA_HD ** (-0.5)
                if m != head:
                    query = pltpu.roll(query, DA_HD, 1)
                query = jnp.where((lane < DA_HD) == (m == 0), query, 0.0).astype(bf16)
                scores = [dot_nt(query, ref[:, :wide]) for ref in blocks]
                scores[0] = jnp.where(causal, scores[0], -1e30)
                for d in range(distances):
                    scores[d + 1] = jnp.where(place > d, scores[d + 1], -1e30)
                top = functools.reduce(jnp.maximum, scores)
                top = jnp.max(top, axis=-1, keepdims=True)
                sums = None
                for part, value in zip(scores, valued):
                    term = dot_nn(jnp.exp(part - top).astype(bf16), value)
                    sums = term if sums is None else sums + term
                maps.append(sums[:, :wide] / sums[:, wide:])
            mixed = maps[0] - lambda_ref[0, head] * maps[1]
            out_ref[rows, head * wide : (head + 1) * wide] = normed(mixed, gain_ref[...])


def attention(query_one, query_two, own, others, weight, gain):
    token_count = query_one.shape[0]
    out = jax.ShapeDtypeStruct((token_count, 2 * query_one.shape[1]), bf16)
    vmem = pl.BlockSpec(memory_space=pltpu.VMEM)
    return pl.pallas_call(
        functools.partial(attention_kernel, len(others)),
        out_shape=out,
        in_specs=[pl.BlockSpec(memory_space=pltpu.SMEM)] + [vmem] * (4 + len(others)),
        out_specs=vmem,
        name="attention",
        compiler_params=PARAMS,
        cost_estimate=cost(
            12 * token_count * token_count * query_one.shape[1] * (1 + len(others)), own, *others
        ),
    )(weight.reshape(1, -1), query_one, query_two, gain.reshape(1, -1), own, *others)


def is_inner():
    place = lax.axis_index("sp")
    return jnp.logical_and(place > 0, place < lax.axis_size("sp") - 1)


def project_kernel(flip, tp_size, counts, *refs):
    mixed_refs, weight_refs, out_ref = refs[:4], list(refs[4:-1]), refs[-1]
    share = mixed_refs[0].shape[0] // tp_size
    place = lax.axis_index("tp")

    def rows_of(ref):
        return [
            ref[pl.ds(pl.multiple_of((place ^ flip ^ across) * share, share), share), :]
            for across in (0, 2)
        ]

    recurrent = jnp.concatenate(rows_of(mixed_refs[0]) + rows_of(mixed_refs[2]), axis=0)
    attended = jnp.concatenate(rows_of(mixed_refs[1]) + rows_of(mixed_refs[3]), axis=0)
    for p, count in enumerate(counts):
        weight = weight_refs.pop(0)[...]
        if count == 2:
            weight = jnp.where(is_inner(), weight_refs.pop(0)[...], weight)
        width = weight.shape[2]
        terms = dot_nn(recurrent, weight[0]) + dot_nn(attended, weight[1])
        out_ref[:, p * width : (p + 1) * width] = terms.astype(out_ref.dtype)


def project(flip, tp_size, mixed, weights, dtype):
    rows = 4 * (mixed[0].shape[0] // tp_size)
    counts = tuple(len(w) for w in weights)
    weights = [w for choice in weights for w in choice]
    out = jax.ShapeDtypeStruct((rows, weights[0].shape[2] * len(counts)), dtype)
    return pl.pallas_call(
        functools.partial(project_kernel, flip, tp_size, counts),
        out_shape=out,
        name="project",
        compiler_params=PARAMS,
        cost_estimate=cost(4 * rows * mixed[0].shape[1] * out.shape[1], *mixed, *weights, out),
    )(*mixed, *weights)


def pair_kernel(kept_ref, came_ref, own_ref, *send_refs):
    share = own_ref.shape[0]
    for k, ref in enumerate((own_ref, *send_refs)):
        rows = slice(k * share, (k + 1) * share)
        ref[...] = (kept_ref[rows, :] + came_ref[rows, :].astype(f32)).astype(ref.dtype)


def pair_sum(kept, came):
    share = (kept.shape[0] // 4, kept.shape[1])
    outs = (jax.ShapeDtypeStruct(share, f32),) + (jax.ShapeDtypeStruct(share, bf16),) * 3
    return pl.pallas_call(
        pair_kernel,
        out_shape=outs,
        name="pair",
        compiler_params=PARAMS,
        cost_estimate=cost(kept.size, kept, came, *outs),
    )(kept, came)


def final_kernel(counts, *refs):
    out_ref = refs[-1]
    group = lax.axis_index("grp")
    place = lax.axis_index("sp")
    turn = jnp.where(is_inner(), 1, 0)
    piece = 0
    for n, count in enumerate(counts):
        own_ref, across_ref, beside_ref, corner_ref = refs[4 * n : 4 * n + 4]
        width = own_ref.shape[1] // count
        for p in range(count):
            lanes = slice(p * width, (p + 1) * width)
            shard = place ^ piece if piece < 2 else place ^ piece ^ turn
            piece += 1
            start = shard * (2 * width)
            mine = own_ref[:, lanes] + across_ref[:, lanes].astype(f32)
            theirs = beside_ref[:, lanes].astype(f32) + corner_ref[:, lanes].astype(f32)
            first = pl.multiple_of(start + group * width, width)
            second = pl.multiple_of(start + (1 - group) * width, width)
            out_ref[:, pl.ds(first, width)] = mine.astype(bf16)
            out_ref[:, pl.ds(second, width)] = theirs.astype(bf16)


def final_sum(pieces, results):
    arrays = [array for result in results for array in result]
    rows = arrays[0].shape[0]
    width = sum(result[0].shape[1] for result in results)
    counts = tuple(pieces * result[0].shape[1] // width for result in results)
    out = jax.ShapeDtypeStruct((rows, 2 * width), bf16)
    return pl.pallas_call(
        functools.partial(final_kernel, counts),
        out_shape=out,
        name="final",
        compiler_params=PARAMS,
        cost_estimate=cost(out.size, *arrays, out),
    )(*arrays)


def fast_shards(
    sizes,
    recurrent_query,
    recurrent_forget_gate,
    recurrent_value,
    recurrent_gate_lower_bound,
    recurrent_added_decay,
    recurrent_norm_gain,
    attention_query_first,
    attention_key_first,
    attention_query_second,
    attention_key_second,
    attention_value,
    second_map_weight,
    attention_norm_gain,
    output_weight,
):
    grp_size, sp_size, tp_size = sizes

    def swap(array, axis, size, d):
        return lax.ppermute(array, axis, [(k, k ^ d) for k in range(size)])

    def up(array, first):
        return lax.ppermute(array, "sp", [(k, k + 1) for k in range(first, sp_size - 1)])

    last = sp_size - 1
    inner = [(k, last - k) for k in range(1, last)]
    outward = [(1, 0), (last - 1, last)]
    own_keys = jnp.concatenate(
        [attention_key_first, attention_key_second, attention_value], axis=1
    )
    key_hops = [own_keys]
    for k in range(last):
        key_hops.append(up(key_hops[-1], k))
    half = output_weight.shape[2] // grp_size
    own_weight = lax.dynamic_slice_in_dim(
        output_weight, lax.axis_index("grp") * half, half, axis=2
    )
    weight_one = swap(own_weight, "sp", sp_size, 1)
    weight_mid = lax.ppermute(own_weight, "sp", inner)
    weight_mid_far = lax.ppermute(weight_one, "sp", inner)
    weight_end = lax.ppermute(weight_mid, "sp", outward)
    weight_end_far = lax.ppermute(weight_mid_far, "sp", outward)
    local, faded, state = local_recurrence(
        recurrent_query,
        recurrent_forget_gate,
        recurrent_value,
        recurrent_gate_lower_bound,
        recurrent_added_decay,
    )
    below = up(state, 0)
    two = merge_states(state, below)
    far = lax.ppermute(two, "sp", [(k, k + 2) for k in range(sp_size - 2)])
    attended = attention(
        attention_query_first,
        attention_query_second,
        own_keys,
        key_hops[1:],
        second_map_weight,
        attention_norm_gain,
    )
    recurrent = carry_in(local, faded, recurrent_norm_gain, (below, far))
    mixed = (
        recurrent, attended, swap(recurrent, "grp", grp_size, 1), swap(attended, "grp", grp_size, 1)
    )
    corner_pairs = [
        (g * tp_size + k, (g ^ 1) * tp_size + (k ^ 2))
        for g in range(grp_size)
        for k in range(tp_size)
    ]
    groups = (
        ((own_weight,), (weight_one,), (weight_end, weight_mid)),
        ((weight_end_far, weight_mid_far),),
    )
    results = []
    for weights in groups:
        sent = project(1, tp_size, mixed, weights, bf16)
        came = swap(sent, "tp", tp_size, 1)
        kept = project(0, tp_size, mixed, weights, f32)
        own, across, beside, corner = pair_sum(kept, came)
        across = swap(across, "tp", tp_size, 2)
        beside = swap(beside, "grp", grp_size, 1)
        corner = lax.ppermute(corner, ("grp", "tp"), corner_pairs)
        results.append((own, across, beside, corner))
    return final_sum(sp_size, results)


def is_short(sizes):
    return sizes == (2, 4, 4)


def shards(sizes, *arrays):
    key_heads = arrays[7].shape[1] // DA_HD
    query_heads = arrays[6].shape[1] // DA_HD
    if is_short(sizes) and key_heads == 1 and query_heads == 2:
        return fast_shards(sizes, *arrays)
    return general_shards(*arrays)


def solution(mesh):
    sizes = (mesh.shape["grp"], mesh.shape["sp"], mesh.shape["tp"])
    return jax.shard_map(
        functools.partial(shards, sizes),
        mesh=mesh,
        in_specs=(
            P(("grp", "sp"), "tp"),
            P(("grp", "sp"), "tp"),
            P(("grp", "sp"), "tp"),
            P("tp"),
            P(("grp", "sp"), "tp"),
            P(),
            P(("grp", "sp"), "tp"),
            P(("grp", "sp"), "tp"),
            P(("grp", "sp"), "tp"),
            P(("grp", "sp"), "tp"),
            P(("grp", "sp"), "tp"),
            P("tp"),
            P(),
            P(None, "tp", "sp"),
        ),
        out_specs=P(("grp", "sp", "tp"), None),
        check_vma=False,
    )
```

profile of v0, /device:TPU:0, one launch (start us, length us, event | category | flops | bytes accessed | tf_op | source)
XLA Modules:
  0.0 67.6 jit_solution(15853546601626106356)
XLA Ops:
  0.0 0.9 %copy.17 = bf16[256,64]{1,0:T(8,128)(2,1)S(1)} copy(bf16[256,64]{0,1:T(8,128)(2,1)} %param.23) | data formatting | bytes 65536 | tf_op args[9]
  1.1 0.7 %copy-done.10 = bf16[256,128]{1,0:T(8,128)(2,1)S(1)} copy-done((bf16[256,128]{1,0:T(8,128)(2,1)S(1)}, bf16[256,128]{1,0:T(8,128)(2,1)}, u32[]{:S(2)}) %copy-start.10) | copy-done | bytes 65560
  1.9 5.0 %collective-permute-start.2 = (bf16[256,256]{1,0:T(8,128)(2,1)S(1)}, bf16[256,256]{1,0:T(8,128)(2,1)S(1)}, u32[]{:S(2)}, u32[]{:S(2)}) collective-permute-start(bf16[256,256]{1,0:T(8,128)(2,1)S(1)} %pad_maximum_fusion.own_ref), channel_id=1, source_target_pairs={{0,4},{4,8},{8,12},{1,5},{5,9},{9,13},{2,6},{6,10},{10,14},{3,7},{... | collective-permute-start | bytes 393224 | tf_op jit(solution)/shard_map/ppermute | solution.py:601
  7.0 0.8 %collective-permute-start.8 = (bf16[2,256,256]{2,1,0:T(8,128)(2,1)S(1)}, bf16[2,256,256]{2,1,0:T(8,128)(2,1)S(1)}, u32[]{:S(2)}, u32[]{:S(2)}) collective-permute-start(bf16[2,256,256]{2,1,0:T(8,128)(2,1)S(1)} %constant_dynamic-slice_fusion.refs_4_), channel_id=1, source_target_pairs={{4,8},{8,4},{5,9},{9,5},{6,10},{10,6},{7,11},{11,7},{20,24},{24,20... | collective-permute-start | bytes 786440 | tf_op jit(solution)/shard_map/ppermute | solution.py:617
  7.8 4.4 %collective-permute-start.7 = (bf16[2,256,256]{2,1,0:T(8,128)(2,1)S(1)}, bf16[2,256,256]{2,1,0:T(8,128)(2,1)S(1)}, u32[]{:S(2)}, u32[]{:S(2)}) collective-permute-start(bf16[2,256,256]{2,1,0:T(8,128)(2,1)S(1)} %constant_dynamic-slice_fusion.refs_4_), channel_id=1, source_target_pairs={{0,4},{4,0},{8,12},{12,8},{1,5},{5,1},{9,13},{13,9},{2,6},{6,2},{1... | collective-permute-start | bytes 786440 | tf_op jit(solution)/shard_map/ppermute | solution.py:598
  13.7 1.1 %recurrence.1 = (f32[256,256]{1,0:T(8,128)S(1)}, bf16[256,256]{1,0:T(8,128)(2,1)S(1)}, bf16[2,144,128]{2,1,0:T(8,128)(2,1)S(1)}) custom-call(bf16[256,256]{1,0:T(8,128)(2,1)S(1)} %copy-done.1, bf16[256,256]{1,0:T(8,128)(2,1)S(1)} %copy-done.2, bf16[256,256]{1,0:T(8,128)(2,1)S(1)} %copy-done.3, f32[1,256]{1,0:T(1,128)S(1)} %bitcast.4, ...), custom_call_target="tpu_custom_call" | custom-call | flops 134217728 | bytes 860160 | tf_op jit(solution)/shard_map/recurrence/pallas_call | solution.py:370
  14.8 4.6 %collective-permute-start = (bf16[2,144,128]{2,1,0:T(8,128)(2,1)S(1)}, bf16[2,144,128]{2,1,0:T(8,128)(2,1)S(1)}, u32[]{:S(2)}, u32[]{:S(2)}) collective-permute-start(bf16[2,144,128]{2,1,0:T(8,128)(2,1)S(1)} %get-tuple-element.18.near_ref), channel_id=1, source_target_pairs={{0,4},{4,8},{8,12},{1,5},{5,9},{9,13},{2,6},{6,10},{10,14},{3,7},{... | collective-permute-start | bytes 221192 | tf_op jit(solution)/shard_map/ppermute | solution.py:601
  19.4 0.7 collective-permute-start.4
  20.1 1.3 %collective-permute-start.9 = (bf16[2,256,256]{2,1,0:T(8,128)(2,1)S(1)}, bf16[2,256,256]{2,1,0:T(8,128)(2,1)S(1)}, u32[]{:S(2)}, u32[]{:S(2)}) collective-permute-start(bf16[2,256,256]{2,1,0:T(8,128)(2,1)S(1)} %collective-permute-done.8.refs_7_), channel_id=1, source_target_pairs={{4,0},{8,12},{5,1},{9,13},{6,2},{10,14},{7,3},{11,15},{20,16},{24,... | collective-permute-start | bytes 786440 | tf_op jit(solution)/shard_map/ppermute | solution.py:619
  21.4 7.6 %collective-permute-start.1 = (bf16[2,144,128]{2,1,0:T(8,128)(2,1)S(1)}, bf16[2,144,128]{2,1,0:T(8,128)(2,1)S(1)}, u32[]{:S(2)}, u32[]{:S(2)}) collective-permute-start(bf16[2,144,128]{2,1,0:T(8,128)(2,1)S(1)} %merge.1), channel_id=1, source_target_pairs={{0,8},{4,12},{1,9},{5,13},{2,10},{6,14},{3,11},{7,15},{16,24},{20,... | collective-permute-start | bytes 221192 | tf_op jit(solution)/shard_map/ppermute | solution.py:630
  29.1 0.7 %collective-permute-start.14 = (bf16[2,256,256]{2,1,0:T(8,128)(2,1)S(1)}, bf16[2,256,256]{2,1,0:T(8,128)(2,1)S(1)}, u32[]{:S(2)}, u32[]{:S(2)}) collective-permute-start(bf16[2,256,256]{2,1,0:T(8,128)(2,1)S(1)} %collective-permute-done.7.refs_5_), channel_id=1, source_target_pairs={{4,8},{8,4},{5,9},{9,5},{6,10},{10,6},{7,11},{11,7},{20,24},{24,20... | collective-permute-start | bytes 786440 | tf_op jit(solution)/shard_map/ppermute | solution.py:618
  29.8 1.3 %collective-permute-done.1.refs_1_ = bf16[2,144,128]{2,1,0:T(8,128)(2,1)S(1)} collective-permute-done((bf16[2,144,128]{2,1,0:T(8,128)(2,1)S(1)}, bf16[2,144,128]{2,1,0:T(8,128)(2,1)S(1)}, u32[]{:S(2)}, u32[]{:S(2)}) %collective-permute-start.1) | collective-permute-done | bytes 73760 | tf_op jit(solution)/shard_map/ppermute | solution.py:630
  32.0 1.6 %collective-permute-start.5 = (bf16[256,256]{1,0:T(8,128)(2,1)S(1)}, bf16[256,256]{1,0:T(8,128)(2,1)S(1)}, u32[]{:S(2)}, u32[]{:S(2)}) collective-permute-start(bf16[256,256]{1,0:T(8,128)(2,1)S(1)} %carry.1.refs_0_), channel_id=1, source_target_pairs={{0,16},{16,0},{1,17},{17,1},{2,18},{18,2},{3,19},{19,3},{4,20},{20... | collective-permute-start | bytes 393224 | tf_op jit(solution)/shard_map/ppermute | solution.py:598
  34.3 2.4 %attention.1.refs_1_ = bf16[256,256]{1,0:T(8,128)(2,1)S(1)} custom-call(f32[1,2]{1,0:T(1,128)S(1)} %bitcast.6, bf16[256,128]{1,0:T(8,128)(2,1)S(1)} %copy-done.6, bf16[256,128]{1,0:T(8,128)(2,1)S(1)} %copy-done.7, f32[1,128]{1,0:T(1,128)S(1)} %bitcast.7, bf16[256,256]{1,0:T(8,128)(2,1)S(1)} %pad_maximum_fusion.own_ref, ...), custom_call_target="tpu_custom_call" | custom-call | flops 402653184 | bytes 524288 | tf_op jit(solution)/shard_map/attention/pallas_call | solution.py:468
  37.8 3.9 %collective-permute-done.6.refs_3_ = bf16[256,256]{1,0:T(8,128)(2,1)S(1)} collective-permute-done((bf16[256,256]{1,0:T(8,128)(2,1)S(1)}, bf16[256,256]{1,0:T(8,128)(2,1)S(1)}, u32[]{:S(2)}, u32[]{:S(2)}) %collective-permute-start.6) | collective-permute-done | bytes 131104 | tf_op jit(solution)/shard_map/ppermute | solution.py:598
  42.2 1.3 %collective-permute-start.15 = (bf16[2,256,256]{2,1,0:T(8,128)(2,1)S(1)}, bf16[2,256,256]{2,1,0:T(8,128)(2,1)S(1)}, u32[]{:S(2)}, u32[]{:S(2)}) collective-permute-start(bf16[2,256,256]{2,1,0:T(8,128)(2,1)S(1)} %collective-permute-done.14.refs_5_), channel_id=1, source_target_pairs={{4,0},{8,12},{5,1},{9,13},{6,2},{10,14},{7,3},{11,15},{20,16},{24,... | collective-permute-start | bytes 786440 | tf_op jit(solution)/shard_map/ppermute | solution.py:620
  43.5 9.3 %collective-permute-done.15.refs_4_ = bf16[2,256,256]{2,1,0:T(8,128)(2,1)S(1)} collective-permute-done((bf16[2,256,256]{2,1,0:T(8,128)(2,1)S(1)}, bf16[2,256,256]{2,1,0:T(8,128)(2,1)S(1)}, u32[]{:S(2)}, u32[]{:S(2)}) %collective-permute-start.15) | collective-permute-done | bytes 262176 | tf_op jit(solution)/shard_map/ppermute | solution.py:620
  53.6 1.6 %collective-permute-start.11 = (bf16[64,768]{1,0:T(8,128)(2,1)S(1)}, bf16[64,768]{1,0:T(8,128)(2,1)S(1)}, u32[]{:S(2)}, u32[]{:S(2)}) collective-permute-start(bf16[64,768]{1,0:T(8,128)(2,1)S(1)} %get-tuple-element.20), channel_id=1, source_target_pairs={{0,2},{1,3},{2,0},{3,1},{4,6},{5,7},{6,4},{7,5},{8,10},{9,11},{10,... | collective-permute-start | bytes 294920 | tf_op jit(solution)/shard_map/ppermute | solution.py:598
  55.7 1.5 %collective-permute-start.13 = (bf16[64,768]{1,0:T(8,128)(2,1)S(1)}, bf16[64,768]{1,0:T(8,128)(2,1)S(1)}, u32[]{:S(2)}, u32[]{:S(2)}) collective-permute-start(bf16[64,768]{1,0:T(8,128)(2,1)S(1)} %get-tuple-element.22), channel_id=1, source_target_pairs={{0,18},{1,19},{2,16},{3,17},{16,2},{17,3},{18,0},{19,1},{4,22},{5,... | collective-permute-start | bytes 294920 | tf_op jit(solution)/shard_map/ppermute | solution.py:660
  57.4 1.6 %collective-permute-start.17 = (bf16[64,256]{1,0:T(8,128)(2,1)S(1)}, bf16[64,256]{1,0:T(8,128)(2,1)S(1)}, u32[]{:S(2)}, u32[]{:S(2)}) collective-permute-start(bf16[64,256]{1,0:T(8,128)(2,1)S(1)} %get-tuple-element.24), channel_id=1, source_target_pairs={{0,2},{1,3},{2,0},{3,1},{4,6},{5,7},{6,4},{7,5},{8,10},{9,11},{10,... | collective-permute-start | bytes 98312 | tf_op jit(solution)/shard_map/ppermute | solution.py:598
  59.5 2.5 %collective-permute-done.17.refs_5_ = bf16[64,256]{1,0:T(8,128)(2,1)S(1)} collective-permute-done((bf16[64,256]{1,0:T(8,128)(2,1)S(1)}, bf16[64,256]{1,0:T(8,128)(2,1)S(1)}, u32[]{:S(2)}, u32[]{:S(2)}) %collective-permute-start.17) | collective-permute-done | bytes 32800 | tf_op jit(solution)/shard_map/ppermute | solution.py:598
  62.0 1.2 %collective-permute-start.19 = (bf16[64,256]{1,0:T(8,128)(2,1)S(1)}, bf16[64,256]{1,0:T(8,128)(2,1)S(1)}, u32[]{:S(2)}, u32[]{:S(2)}) collective-permute-start(bf16[64,256]{1,0:T(8,128)(2,1)S(1)} %get-tuple-element.26), channel_id=1, source_target_pairs={{0,18},{1,19},{2,16},{3,17},{16,2},{17,3},{18,0},{19,1},{4,22},{5,... | collective-permute-start | bytes 98312 | tf_op jit(solution)/shard_map/ppermute | solution.py:660
  63.2 3.6 %collective-permute-done.19.refs_7_ = bf16[64,256]{1,0:T(8,128)(2,1)S(1)} collective-permute-done((bf16[64,256]{1,0:T(8,128)(2,1)S(1)}, bf16[64,256]{1,0:T(8,128)(2,1)S(1)}, u32[]{:S(2)}, u32[]{:S(2)}) %collective-permute-start.19) | collective-permute-done | bytes 32800 | tf_op jit(solution)/shard_map/ppermute | solution.py:660
  66.8 0.8 %final.1 = bf16[64,2048]{1,0:T(8,128)(2,1)} custom-call(f32[64,768]{1,0:T(8,128)S(1)} %get-tuple-element.19.refs_0_, bf16[64,768]{1,0:T(8,128)(2,1)S(1)} %collective-permute-done.11.refs_1_, bf16[64,768]{1,0:T(8,128)(2,1)S(1)} %collective-permute-done.12.refs_2_, bf16[64,768]{1,0:T(8,128)(2,1)S(1)} %collective-permute-done.13.refs_3_, ...), custom_call_target="tpu_custom_call" | custom-call | flops 131072 | bytes 917504 | tf_op jit(solution)/shard_map/final/pallas_call | solution.py:569
  (58 shorter events, 7.0 us)
Async XLA Ops:
  0.0 6.9 %copy-start = (bf16[2,256,512]{2,1,0:T(8,128)(2,1)S(1)}, bf16[2,256,512]{2,1,0:T(8,128)(2,1)}, u32[]{:S(2)}) copy-start(bf16[2,256,512]{2,1,0:T(8,128)(2,1)} %param.27) | copy-start | bytes 1572868
  1.9 10.3 %collective-permute-start.2 = (bf16[256,256]{1,0:T(8,128)(2,1)S(1)}, bf16[256,256]{1,0:T(8,128)(2,1)S(1)}, u32[]{:S(2)}, u32[]{:S(2)}) collective-permute-start(bf16[256,256]{1,0:T(8,128)(2,1)S(1)} %pad_maximum_fusion.own_ref), channel_id=1, source_target_pairs={{0,4},{4,8},{8,12},{1,5},{5,9},{9,13},{2,6},{6,10},{10,14},{3,7},{... | collective-permute-start | bytes 393224 | tf_op jit(solution)/shard_map/ppermute | solution.py:601
  6.9 6.2 %copy-start.2 = (bf16[256,256]{1,0:T(8,128)(2,1)S(1)}, bf16[256,256]{1,0:T(8,128)(2,1)}, u32[]{:S(2)}) copy-start(bf16[256,256]{1,0:T(8,128)(2,1)} %gate_ref.1) | copy-start | bytes 393220
  6.9 6.2 %copy-start.3 = (bf16[256,256]{1,0:T(8,128)(2,1)S(1)}, bf16[256,256]{1,0:T(8,128)(2,1)}, u32[]{:S(2)}) copy-start(bf16[256,256]{1,0:T(8,128)(2,1)} %value_ref.1) | copy-start | bytes 393220
  7.0 6.1 %copy-start.1 = (bf16[256,256]{1,0:T(8,128)(2,1)S(1)}, bf16[256,256]{1,0:T(8,128)(2,1)}, u32[]{:S(2)}) copy-start(bf16[256,256]{1,0:T(8,128)(2,1)} %query_ref.1) | copy-start | bytes 393220
  7.0 13.1 %collective-permute-start.8 = (bf16[2,256,256]{2,1,0:T(8,128)(2,1)S(1)}, bf16[2,256,256]{2,1,0:T(8,128)(2,1)S(1)}, u32[]{:S(2)}, u32[]{:S(2)}) collective-permute-start(bf16[2,256,256]{2,1,0:T(8,128)(2,1)S(1)} %constant_dynamic-slice_fusion.refs_4_), channel_id=1, source_target_pairs={{4,8},{8,4},{5,9},{9,5},{6,10},{10,6},{7,11},{11,7},{20,24},{24,20... | collective-permute-start | bytes 786440 | tf_op jit(solution)/shard_map/ppermute | solution.py:617
  7.8 21.3 %collective-permute-start.7 = (bf16[2,256,256]{2,1,0:T(8,128)(2,1)S(1)}, bf16[2,256,256]{2,1,0:T(8,128)(2,1)S(1)}, u32[]{:S(2)}, u32[]{:S(2)}) collective-permute-start(bf16[2,256,256]{2,1,0:T(8,128)(2,1)S(1)} %constant_dynamic-slice_fusion.refs_4_), channel_id=1, source_target_pairs={{0,4},{4,0},{8,12},{12,8},{1,5},{5,1},{9,13},{13,9},{2,6},{6,2},{1... | collective-permute-start | bytes 786440 | tf_op jit(solution)/shard_map/ppermute | solution.py:598
  12.2 7.2 %collective-permute-start.3 = (bf16[256,256]{1,0:T(8,128)(2,1)S(1)}, bf16[256,256]{1,0:T(8,128)(2,1)S(1)}, u32[]{:S(2)}, u32[]{:S(2)}) collective-permute-start(bf16[256,256]{1,0:T(8,128)(2,1)S(1)} %collective-permute-done.2.refs_0_), channel_id=1, source_target_pairs={{4,8},{8,12},{5,9},{9,13},{6,10},{10,14},{7,11},{11,15},{20,24},{2... | collective-permute-start | bytes 393224 | tf_op jit(solution)/shard_map/ppermute | solution.py:601
  14.8 6.6 %collective-permute-start = (bf16[2,144,128]{2,1,0:T(8,128)(2,1)S(1)}, bf16[2,144,128]{2,1,0:T(8,128)(2,1)S(1)}, u32[]{:S(2)}, u32[]{:S(2)}) collective-permute-start(bf16[2,144,128]{2,1,0:T(8,128)(2,1)S(1)} %get-tuple-element.18.near_ref), channel_id=1, source_target_pairs={{0,4},{4,8},{8,12},{1,5},{5,9},{9,13},{2,6},{6,10},{10,14},{3,7},{... | collective-permute-start | bytes 221192 | tf_op jit(solution)/shard_map/ppermute | solution.py:601
  19.4 14.2 %collective-permute-start.4 = (bf16[256,256]{1,0:T(8,128)(2,1)S(1)}, bf16[256,256]{1,0:T(8,128)(2,1)S(1)}, u32[]{:S(2)}, u32[]{:S(2)}) collective-permute-start(bf16[256,256]{1,0:T(8,128)(2,1)S(1)} %collective-permute-done.3.refs_1_), channel_id=1, source_target_pairs={{8,12},{9,13},{10,14},{11,15},{24,28},{25,29},{26,30},{27,31}} | collective-permute-start | bytes 393224 | tf_op jit(solution)/shard_map/ppermute | solution.py:601
  20.1 21.7 %collective-permute-start.9 = (bf16[2,256,256]{2,1,0:T(8,128)(2,1)S(1)}, bf16[2,256,256]{2,1,0:T(8,128)(2,1)S(1)}, u32[]{:S(2)}, u32[]{:S(2)}) collective-permute-start(bf16[2,256,256]{2,1,0:T(8,128)(2,1)S(1)} %collective-permute-done.8.refs_7_), channel_id=1, source_target_pairs={{4,0},{8,12},{5,1},{9,13},{6,2},{10,14},{7,3},{11,15},{20,16},{24,... | collective-permute-start | bytes 786440 | tf_op jit(solution)/shard_map/ppermute | solution.py:619
  21.4 9.6 %collective-permute-start.1 = (bf16[2,144,128]{2,1,0:T(8,128)(2,1)S(1)}, bf16[2,144,128]{2,1,0:T(8,128)(2,1)S(1)}, u32[]{:S(2)}, u32[]{:S(2)}) collective-permute-start(bf16[2,144,128]{2,1,0:T(8,128)(2,1)S(1)} %merge.1), channel_id=1, source_target_pairs={{0,8},{4,12},{1,9},{5,13},{2,10},{6,14},{3,11},{7,15},{16,24},{20,... | collective-permute-start | bytes 221192 | tf_op jit(solution)/shard_map/ppermute | solution.py:630
  29.1 13.1 %collective-permute-start.14 = (bf16[2,256,256]{2,1,0:T(8,128)(2,1)S(1)}, bf16[2,256,256]{2,1,0:T(8,128)(2,1)S(1)}, u32[]{:S(2)}, u32[]{:S(2)}) collective-permute-start(bf16[2,256,256]{2,1,0:T(8,128)(2,1)S(1)} %collective-permute-done.7.refs_5_), channel_id=1, source_target_pairs={{4,8},{8,4},{5,9},{9,5},{6,10},{10,6},{7,11},{11,7},{20,24},{24,20... | collective-permute-start | bytes 786440 | tf_op jit(solution)/shard_map/ppermute | solution.py:618
  32.0 5.8 %collective-permute-start.5 = (bf16[256,256]{1,0:T(8,128)(2,1)S(1)}, bf16[256,256]{1,0:T(8,128)(2,1)S(1)}, u32[]{:S(2)}, u32[]{:S(2)}) collective-permute-start(bf16[256,256]{1,0:T(8,128)(2,1)S(1)} %carry.1.refs_0_), channel_id=1, source_target_pairs={{0,16},{16,0},{1,17},{17,1},{2,18},{18,2},{3,19},{19,3},{4,20},{20... | collective-permute-start | bytes 393224 | tf_op jit(solution)/shard_map/ppermute | solution.py:598
  36.7 5.0 %collective-permute-start.6 = (bf16[256,256]{1,0:T(8,128)(2,1)S(1)}, bf16[256,256]{1,0:T(8,128)(2,1)S(1)}, u32[]{:S(2)}, u32[]{:S(2)}) collective-permute-start(bf16[256,256]{1,0:T(8,128)(2,1)S(1)} %attention.1.refs_1_), channel_id=1, source_target_pairs={{0,16},{16,0},{1,17},{17,1},{2,18},{18,2},{3,19},{19,3},{4,20},{20... | collective-permute-start | bytes 393224 | tf_op jit(solution)/shard_map/ppermute | solution.py:598
  42.1 11.4 %collective-permute-start.10 = (bf16[256,768]{1,0:T(8,128)(2,1)S(1)}, bf16[256,768]{1,0:T(8,128)(2,1)S(1)}, u32[]{:S(2)}, u32[]{:S(2)}) collective-permute-start(bf16[256,768]{1,0:T(8,128)(2,1)S(1)} %project.5), channel_id=1, source_target_pairs={{0,1},{1,0},{2,3},{3,2},{4,5},{5,4},{6,7},{7,6},{8,9},{9,8},{10,11... | collective-permute-start | bytes 1179656 | tf_op jit(solution)/shard_map/ppermute | solution.py:598
  42.2 10.6 %collective-permute-start.15 = (bf16[2,256,256]{2,1,0:T(8,128)(2,1)S(1)}, bf16[2,256,256]{2,1,0:T(8,128)(2,1)S(1)}, u32[]{:S(2)}, u32[]{:S(2)}) collective-permute-start(bf16[2,256,256]{2,1,0:T(8,128)(2,1)S(1)} %collective-permute-done.14.refs_5_), channel_id=1, source_target_pairs={{4,0},{8,12},{5,1},{9,13},{6,2},{10,14},{7,3},{11,15},{20,16},{24,... | collective-permute-start | bytes 786440 | tf_op jit(solution)/shard_map/ppermute | solution.py:620
  53.1 4.3 %collective-permute-start.16 = (bf16[256,256]{1,0:T(8,128)(2,1)S(1)}, bf16[256,256]{1,0:T(8,128)(2,1)S(1)}, u32[]{:S(2)}, u32[]{:S(2)}) collective-permute-start(bf16[256,256]{1,0:T(8,128)(2,1)S(1)} %project.7), channel_id=1, source_target_pairs={{0,1},{1,0},{2,3},{3,2},{4,5},{5,4},{6,7},{7,6},{8,9},{9,8},{10,11... | collective-permute-start | bytes 393224 | tf_op jit(solution)/shard_map/ppermute | solution.py:598
  53.6 13.2 %collective-permute-start.11 = (bf16[64,768]{1,0:T(8,128)(2,1)S(1)}, bf16[64,768]{1,0:T(8,128)(2,1)S(1)}, u32[]{:S(2)}, u32[]{:S(2)}) collective-permute-start(bf16[64,768]{1,0:T(8,128)(2,1)S(1)} %get-tuple-element.20), channel_id=1, source_target_pairs={{0,2},{1,3},{2,0},{3,1},{4,6},{5,7},{6,4},{7,5},{8,10},{9,11},{10,... | collective-permute-start | bytes 294920 | tf_op jit(solution)/shard_map/ppermute | solution.py:598
  55.2 11.6 %collective-permute-start.12 = (bf16[64,768]{1,0:T(8,128)(2,1)S(1)}, bf16[64,768]{1,0:T(8,128)(2,1)S(1)}, u32[]{:S(2)}, u32[]{:S(2)}) collective-permute-start(bf16[64,768]{1,0:T(8,128)(2,1)S(1)} %get-tuple-element.21), channel_id=1, source_target_pairs={{0,16},{16,0},{1,17},{17,1},{2,18},{18,2},{3,19},{19,3},{4,20},{20... | collective-permute-start | bytes 294920 | tf_op jit(solution)/shard_map/ppermute | solution.py:598
  55.7 11.1 %collective-permute-start.13 = (bf16[64,768]{1,0:T(8,128)(2,1)S(1)}, bf16[64,768]{1,0:T(8,128)(2,1)S(1)}, u32[]{:S(2)}, u32[]{:S(2)}) collective-permute-start(bf16[64,768]{1,0:T(8,128)(2,1)S(1)} %get-tuple-element.22), channel_id=1, source_target_pairs={{0,18},{1,19},{2,16},{3,17},{16,2},{17,3},{18,0},{19,1},{4,22},{5,... | collective-permute-start | bytes 294920 | tf_op jit(solution)/shard_map/ppermute | solution.py:660
  57.4 4.5 %collective-permute-start.17 = (bf16[64,256]{1,0:T(8,128)(2,1)S(1)}, bf16[64,256]{1,0:T(8,128)(2,1)S(1)}, u32[]{:S(2)}, u32[]{:S(2)}) collective-permute-start(bf16[64,256]{1,0:T(8,128)(2,1)S(1)} %get-tuple-element.24), channel_id=1, source_target_pairs={{0,2},{1,3},{2,0},{3,1},{4,6},{5,7},{6,4},{7,5},{8,10},{9,11},{10,... | collective-permute-start | bytes 98312 | tf_op jit(solution)/shard_map/ppermute | solution.py:598
  59.0 4.2 %collective-permute-start.18 = (bf16[64,256]{1,0:T(8,128)(2,1)S(1)}, bf16[64,256]{1,0:T(8,128)(2,1)S(1)}, u32[]{:S(2)}, u32[]{:S(2)}) collective-permute-start(bf16[64,256]{1,0:T(8,128)(2,1)S(1)} %get-tuple-element.25), channel_id=1, source_target_pairs={{0,16},{16,0},{1,17},{17,1},{2,18},{18,2},{3,19},{19,3},{4,20},{20... | collective-permute-start | bytes 98312 | tf_op jit(solution)/shard_map/ppermute | solution.py:598
  62.0 4.8 %collective-permute-start.19 = (bf16[64,256]{1,0:T(8,128)(2,1)S(1)}, bf16[64,256]{1,0:T(8,128)(2,1)S(1)}, u32[]{:S(2)}, u32[]{:S(2)}) collective-permute-start(bf16[64,256]{1,0:T(8,128)(2,1)S(1)} %get-tuple-element.26), channel_id=1, source_target_pairs={{0,18},{1,19},{2,16},{3,17},{16,2},{17,3},{18,0},{19,1},{4,22},{5,... | collective-permute-start | bytes 98312 | tf_op jit(solution)/shard_map/ppermute | solution.py:660
  (9 other events, 14.3 us)
where the time goes:
time: 68 us; the launch traced here: 67.6 us
  starting transfers between devices  36.1 us (53%)
  waiting for transfers between devices  21.1 us (31%)
  Pallas kernels  5.91 us (9%)
  local copies, waits for them, and re-layouts  3.92 us (6%)
    ppermute x4, starting transfers between devices, up(): lax.ppermute(array, 'sp', [(k, k + 1) for k in range(first, sp_size - 1)])  10.9 us
    ppermute x9, starting transfers between devices, swap(): return lax.ppermute(array, axis, [(k, k ^ d) for k in range(size)])  10.9 us
    ppermute x1, waiting for transfers between devices, fast_shards(): weight_end_far = lax.ppermute(weight_mid_far, 'sp', outward)  9.28 us
    ppermute x1, starting transfers between devices, fast_shards(): far = lax.ppermute(two, 'sp', [(k, k + 2) for k in range(sp_size - 2)])  7.63 us
    ppermute x9, waiting for transfers between devices, swap(): return lax.ppermute(array, axis, [(k, k ^ d) for k in range(size)])  6.94 us
    unnamed x29, local copies, waits for them, and re-layouts  3.89 us
    ppermute x2, waiting for transfers between devices, fast_shards(): corner = lax.ppermute(corner, ('grp', 'tp'), corner_pairs)  3.63 us
    ppermute x2, starting transfers between devices, fast_shards(): corner = lax.ppermute(corner, ('grp', 'tp'), corner_pairs)  2.67 us
  transfers between devices with their start and end apart: 20, of which 6 were waited for; matrix products, arithmetic and copies ran while one was open for 0% of the time, Pallas kernels for 8%

commit v1 on v0

--- a/solution.py
+++ b/solution.py
@@ -302,17 +302,47 @@
     return pl.CostEstimate(flops=flops, bytes_accessed=moved, transcendentals=0)
 
 
-def recurrence_kernel(
-    query_ref, gate_ref, value_ref, bound_ref, added_ref, local_ref, faded_ref, state_ref
-):
+BASE = 4 * DA_HD
+STATE = slice(BASE, BASE + HG_DV)
+FADE = slice(BASE + HG_DV, BASE + HG_DV + SPARE_ROWS)
+HBM = pl.BlockSpec(memory_space=pltpu.HBM)
+VMEM = pl.BlockSpec(memory_space=pltpu.VMEM)
+
+
+def prepare_kernel(last, *refs):
+    sources, rest = refs[:13], refs[13:]
+    local_ref, faded_ref, packed_ref, front_ref, asked_ref, gain_ref, weight_ref = rest[:7]
+    query_ref, gate_ref, value_ref, bound_ref, added_ref, lift_ref, sems = rest[7:]
     token_count, width = query_ref.shape
     heads = width // HG_DK
-    chunk = min(token_count, HG_DK)
+    chunk = HG_DK
+    wide = 2 * DA_HD
+    targets = [
+        packed_ref.at[:DA_HD, :],
+        packed_ref.at[DA_HD:wide, :],
+        lift_ref,
+        asked_ref.at[:, :wide],
+        asked_ref.at[:, wide:],
+        gate_ref,
+        bound_ref,
+        added_ref,
+        query_ref,
+        value_ref,
+        gain_ref.at[0:1, :],
+        gain_ref.at[1:2, :],
+        weight_ref,
+    ]
+    copies = [
+        pltpu.make_async_copy(source, target, sems.at[k])
+        for k, (source, target) in enumerate(zip(sources, targets))
+    ]
+    for copy in copies:
+        copy.start()
+    for copy in copies[5:]:
+        copy.wait()
     floor_rate = jax.nn.sigmoid(-bound_ref[...])
     inflow = floor_rate * jax.nn.sigmoid(-gate_ref[...].astype(f32))
-    added = added_ref[...]
-    wide = [jnp.broadcast_to(added[:, h : h + 1], (token_count, HG_DK)) for h in range(heads)]
-    log_decay = jnp.log1p(-inflow) + jnp.concatenate(wide, axis=1)
+    log_decay = jnp.log1p(-inflow)
     row = lax.broadcasted_iota(jnp.int32, (chunk, chunk), 0)
     column = lax.broadcasted_iota(jnp.int32, (chunk, chunk), 1)
     causal = row >= column
@@ -324,19 +354,24 @@
         steps = log_decay[rows]
         coarse = steps.astype(bf16)
         fine = (steps - coarse.astype(f32)).astype(bf16)
-        summed = dot_nn(lower, coarse) + dot_nn(lower, fine)
-        last = summed[chunk - 1 : chunk]
+        extra = []
+        for h in range(heads):
+            steps_row = jnp.where(causal, added_ref[h : h + 1, rows], 0.0)
+            extra.append(
+                jnp.broadcast_to(jnp.sum(steps_row, axis=1, keepdims=True), (chunk, HG_DK))
+            )
+        summed = dot_nn(lower, coarse) + dot_nn(lower, fine) + jnp.concatenate(extra, axis=1)
+        final = summed[chunk - 1 : chunk]
         middle = summed[chunk // 2 - 1 : chunk // 2]
         query = query_ref[rows, :].astype(f32)
         inflow_rows = inflow[rows]
         near_query = (query * jnp.exp(summed - middle)).astype(bf16)
         near_key = (inflow_rows * jnp.exp(middle - summed)).astype(bf16)
-        tail_key = (inflow_rows * jnp.exp(last - summed)).astype(bf16)
-        faded = (query * jnp.exp(summed + total)).astype(bf16)
-        faded_ref[rows, :] = faded
+        tail_key = (inflow_rows * jnp.exp(final - summed)).astype(bf16)
+        faded_ref[rows, :] = (query * jnp.exp(summed + total)).astype(bf16)
         if n:
             base_query = (query * jnp.exp(summed)).astype(bf16)
-        fade = jnp.exp(last)
+        fade = jnp.exp(final)
         for h in range(heads):
             lanes = slice(h * HG_DK, (h + 1) * HG_DK)
             value = value_ref[rows, lanes]
@@ -349,31 +384,91 @@
                 grown = grown + states[h] * fade[:, lanes]
             states[h] = grown
             local_ref[rows, lanes] = out
-        total = total + last
+        total = total + final
     through = jnp.exp(total)
     for h in range(heads):
         lanes = slice(h * HG_DK, (h + 1) * HG_DK)
-        state_ref[h, :HG_DV, :] = states[h].astype(bf16)
-        state_ref[h, HG_DV:, :] = jnp.broadcast_to(through[:, lanes], (SPARE_ROWS, HG_DK)).astype(
-            bf16
-        )
-
-
-def local_recurrence(query, gate, value, bound, added):
+        packed_ref[STATE, lanes] = states[h].astype(bf16)
+    packed_ref[FADE, :] = jnp.broadcast_to(through, (SPARE_ROWS, width)).astype(bf16)
+    for copy in copies[:5]:
+        copy.wait()
+    for n in range(token_count // wide):
+        block = lift_ref[n * wide : (n + 1) * wide, :]
+        packed_ref[wide:BASE, n * wide : (n + 1) * wide] = block
+    front_ref[:BASE, :] = packed_ref[:BASE, :]
+    at_end = lax.axis_index("sp") == last
+
+    @pl.when(at_end)
+    def _():
+        front_ref[BASE:, :] = asked_ref[...]
+
+    @pl.when(jnp.logical_not(at_end))
+    def _():
+        front_ref[BASE : BASE + HG_DV + SPARE_ROWS, :] = packed_ref[BASE:, :]
+
+
+def prepare(last, arrays):
+    (
+        query,
+        gate,
+        value,
+        bound,
+        added,
+        gain,
+        query_one,
+        key_one,
+        query_two,
+        key_two,
+        att_value,
+        weight,
+        att_gain,
+    ) = arrays
     token_count, width = query.shape
-    heads = width // HG_DK
+    wide = 2 * DA_HD
+    rows = BASE + HG_DV + SPARE_ROWS
+    shape = jax.ShapeDtypeStruct
     outs = (
-        jax.ShapeDtypeStruct((token_count, width), f32),
-        jax.ShapeDtypeStruct((token_count, width), bf16),
-        jax.ShapeDtypeStruct((heads, HG_DV + SPARE_ROWS, HG_DK), bf16),
+        shape((token_count, width), f32),
+        shape((token_count, width), bf16),
+        shape((rows, width), bf16),
+        shape((BASE + token_count, width), bf16),
+        shape((token_count, width), bf16),
+        shape((2, HG_DV), f32),
+        shape((1, weight.shape[0]), f32),
+    )
+    inputs = (
+        key_one.T,
+        key_two.T,
+        att_value,
+        query_one,
+        query_two,
+        gate,
+        bound.reshape(1, -1),
+        added.T,
+        query,
+        value,
+        gain.reshape(1, -1),
+        att_gain.reshape(1, -1),
+        weight.reshape(1, -1),
     )
     return pl.pallas_call(
-        recurrence_kernel,
+        functools.partial(prepare_kernel, last),
         out_shape=outs,
-        name="recurrence",
+        in_specs=[HBM] * len(inputs),
+        out_specs=[VMEM] * len(outs),
+        scratch_shapes=[
+            pltpu.VMEM((token_count, width), bf16),
+            pltpu.VMEM((token_count, width), bf16),
+            pltpu.VMEM((token_count, width), bf16),
+            pltpu.VMEM((1, width), f32),
+            pltpu.VMEM(added.T.shape, f32),
+            pltpu.VMEM((token_count, wide), bf16),
+            pltpu.SemaphoreType.DMA((len(inputs),)),
+        ],
+        name="prepare",
         compiler_params=PARAMS,
         cost_estimate=cost(16 * token_count * width * HG_DK, query, gate, value, *outs),
-    )(query, gate, value, bound.reshape(1, -1), added)
+    )(*(pltpu.with_memory_space_constraint(array, pltpu.HBM) for array in inputs))
 
 
 def normed(values, gain):
@@ -381,59 +476,62 @@
     return (values * lax.rsqrt(mean_square + epsilon) * gain).astype(bf16)
 
 
-def carry_kernel(distances, local_ref, faded_ref, gain_ref, *refs):
-    state_refs, out_ref = refs[:distances], refs[distances]
+def blend_kernel(own_ref, one_ref, two_ref, out_ref):
+    merged = one_ref[STATE, :].astype(f32)
+    merged = merged + fade_of(one_ref) * two_ref[STATE, :].astype(f32)
+    merged = own_ref[STATE, :].astype(f32) + fade_of(own_ref) * merged
+    out_ref[...] = merged.astype(bf16)
+
+
+def fade_of(ref):
+    return ref[BASE + HG_DV : BASE + HG_DV + 1, :].astype(f32)
+
+
+def blend(own, one, two):
+    return pl.pallas_call(
+        blend_kernel,
+        out_shape=jax.ShapeDtypeStruct((HG_DV, own.shape[1]), bf16),
+        name="blend",
+        compiler_params=PARAMS,
+        cost_estimate=cost(own.size, own, one, two),
+    )(own, one, two)
+
+
+def carry_kernel(local_ref, faded_ref, gain_ref, p1_ref, p2_ref, p3_ref, p4_ref, out_ref):
     heads = local_ref.shape[1] // HG_DV
+    place = lax.axis_index("sp")
+    merged = p2_ref[STATE, :].astype(f32) + fade_of(p2_ref) * p3_ref[STATE, :].astype(f32)
+    incoming = jnp.where(place == 2, merged, p4_ref[...].astype(f32))
+    incoming = jnp.where(place == 1, p1_ref[STATE, :].astype(f32), incoming)
+    incoming = jnp.where(place == 0, 0.0, incoming).astype(bf16)
     for h in range(heads):
         lanes = slice(h * HG_DV, (h + 1) * HG_DV)
-        incoming = jnp.zeros((HG_DV, HG_DK), f32)
-        for ref in reversed(state_refs):
-            through = ref[h, HG_DV : HG_DV + 1, :].astype(f32)
-            incoming = ref[h, :HG_DV, :].astype(f32) + through * incoming
-        mixed = local_ref[:, lanes] + dot_nt(faded_ref[:, lanes], incoming.astype(bf16))
-        out_ref[:, lanes] = normed(mixed, gain_ref[...])
-
-
-def merge_kernel(near_ref, far_ref, out_ref):
-    for h in range(near_ref.shape[0]):
-        through = near_ref[h, HG_DV : HG_DV + 1, :].astype(f32)
-        merged = near_ref[h].astype(f32) + through * far_ref[h].astype(f32)
-        fade = through * far_ref[h, HG_DV:, :].astype(f32)
-        out_ref[h, :HG_DV, :] = merged[:HG_DV].astype(bf16)
-        out_ref[h, HG_DV:, :] = fade.astype(bf16)
-
-
-def merge_states(near, far):
+        mixed = local_ref[:, lanes] + dot_nt(faded_ref[:, lanes], incoming[:, lanes])
+        out_ref[:, lanes] = normed(mixed, gain_ref[0:1, :])
+
+
+def carry_in(local, faded, gain, *parts):
     return pl.pallas_call(
-        merge_kernel,
-        out_shape=jax.ShapeDtypeStruct(near.shape, bf16),
-        name="merge",
-        compiler_params=PARAMS,
-        cost_estimate=cost(3 * near.size, near, far),
-    )(near, far)
-
-
-def carry_in(local, faded, gain, states):
-    out = jax.ShapeDtypeStruct(local.shape, bf16)
-    return pl.pallas_call(
-        functools.partial(carry_kernel, len(states)),
-        out_shape=out,
+        carry_kernel,
+        out_shape=jax.ShapeDtypeStruct(local.shape, bf16),
         name="carry",
         compiler_params=PARAMS,
-        cost_estimate=cost(4 * local.size * HG_DK, local, faded, *states),
-    )(local, faded, gain.reshape(1, -1), *states)
-
-
-def attention_kernel(distances, lambda_ref, one_ref, two_ref, gain_ref, own_ref, *refs):
-    other_refs, out_ref = refs[:distances], refs[distances]
-    token_count = one_ref.shape[0]
-    place = lax.axis_index("sp")
-    tile = min(token_count, 2 * DA_HD)
-    lane = lax.broadcasted_iota(jnp.int32, (tile, 2 * DA_HD), 1)
-    blocks = (own_ref, *other_refs)
+        cost_estimate=cost(4 * local.size * HG_DK, local, faded, *parts),
+    )(local, faded, gain, *parts)
+
+
+def attend(asked, blocks, weight_ref, gain_ref, out_ref):
     wide = 2 * DA_HD
+    token_count = asked.shape[0]
+    tile = min(token_count, wide)
+    lane = lax.broadcasted_iota(jnp.int32, (tile, wide), 1)
     ones = jnp.ones((token_count, wide), bf16)
-    valued = [jnp.concatenate([ref[:, wide : 2 * wide], ones], axis=1) for ref in blocks]
+    valued = []
+    for ref, _ in blocks:
+        value = [
+            ref[wide:BASE, n * wide : (n + 1) * wide] for n in range(token_count // wide)
+        ]
+        valued.append(jnp.concatenate([jnp.concatenate(value, axis=0), ones], axis=1))
     for t in range(token_count // tile):
         rows = slice(t * tile, (t + 1) * tile)
         row = lax.broadcasted_iota(jnp.int32, (tile, token_count), 0) + t * tile
@@ -441,15 +539,19 @@
         causal = row >= column
         for head in range(2):
             maps = []
-            for m, ref in enumerate((one_ref, two_ref)):
-                query = ref[rows, :].astype(f32) * DA_HD ** (-0.5)
+            for m in range(2):
+                query = asked[rows, m * wide : (m + 1) * wide].astype(f32) * DA_HD ** (-0.5)
                 if m != head:
                     query = pltpu.roll(query, DA_HD, 1)
                 query = jnp.where((lane < DA_HD) == (m == 0), query, 0.0).astype(bf16)
-                scores = [dot_nt(query, ref[:, :wide]) for ref in blocks]
-                scores[0] = jnp.where(causal, scores[0], -1e30)
-                for d in range(distances):
-                    scores[d + 1] = jnp.where(place > d, scores[d + 1], -1e30)
+                scores = []
+                for ref, allowed in blocks:
+                    score = dot_nn(query, ref[:wide, :])
+                    if allowed is None:
+                        score = jnp.where(causal, score, -1e30)
+                    elif allowed is not True:
+                        score = jnp.where(allowed, score, -1e30)
+                    scores.append(score)
                 top = functools.reduce(jnp.maximum, scores)
                 top = jnp.max(top, axis=-1, keepdims=True)
                 sums = None
@@ -457,25 +559,61 @@
                     term = dot_nn(jnp.exp(part - top).astype(bf16), value)
                     sums = term if sums is None else sums + term
                 maps.append(sums[:, :wide] / sums[:, wide:])
-            mixed = maps[0] - lambda_ref[0, head] * maps[1]
-            out_ref[rows, head * wide : (head + 1) * wide] = normed(mixed, gain_ref[...])
-
-
-def attention(query_one, query_two, own, others, weight, gain):
-    token_count = query_one.shape[0]
-    out = jax.ShapeDtypeStruct((token_count, 2 * query_one.shape[1]), bf16)
-    vmem = pl.BlockSpec(memory_space=pltpu.VMEM)
+            mixed = maps[0] - weight_ref[0:1, head : head + 1] * maps[1]
+            out_ref[rows, head * wide : (head + 1) * wide] = normed(mixed, gain_ref[1:2, :])
+
+
+def helper_kernel(last, own_ref, p1_ref, p2_ref, p3_ref, weight_ref, gain_ref, out_ref):
+    @pl.when(lax.axis_index("sp") == last - 1)
+    def _():
+        blocks = [(p1_ref, None), (own_ref, True), (p2_ref, True), (p3_ref, True)]
+        attend(p1_ref.at[BASE:, :], blocks, weight_ref, gain_ref, out_ref)
+
+
+def main_kernel(last, asked_ref, own_ref, p1_ref, p2_ref, p3_ref, weight_ref, gain_ref, out_ref):
+    place = lax.axis_index("sp")
+
+    @pl.when(place == last - 1)
+    def _():
+        blocks = [(own_ref, None), (p2_ref, True), (p3_ref, True)]
+        attend(asked_ref, blocks, weight_ref, gain_ref, out_ref)
+
+    @pl.when(place < last - 1)
+    def _():
+        blocks = [(own_ref, None), (p1_ref, place > 0)]
+        attend(asked_ref, blocks, weight_ref, gain_ref, out_ref)
+
+
+def attention(kernel, last, token_count, *arrays):
+    width = arrays[0].shape[1]
     return pl.pallas_call(
-        functools.partial(attention_kernel, len(others)),
-        out_shape=out,
-        in_specs=[pl.BlockSpec(memory_space=pltpu.SMEM)] + [vmem] * (4 + len(others)),
-        out_specs=vmem,
-        name="attention",
+        functools.partial(kernel, last),
+        out_shape=jax.ShapeDtypeStruct((token_count, width), bf16),
         compiler_params=PARAMS,
-        cost_estimate=cost(
-            12 * token_count * token_count * query_one.shape[1] * (1 + len(others)), own, *others
-        ),
-    )(weight.reshape(1, -1), query_one, query_two, gain.reshape(1, -1), own, *others)
+        cost_estimate=cost(24 * token_count * token_count * width, *arrays),
+    )(*arrays)
+
+
+def choose_kernel(last, main_ref, helped_ref, out_ref):
+    at_end = lax.axis_index("sp") == last
+
+    @pl.when(at_end)
+    def _():
+        out_ref[...] = helped_ref[...]
+
+    @pl.when(jnp.logical_not(at_end))
+    def _():
+        out_ref[...] = main_ref[...]
+
+
+def choose(last, main, helped):
+    return pl.pallas_call(
+        functools.partial(choose_kernel, last),
+        out_shape=jax.ShapeDtypeStruct(main.shape, bf16),
+        name="choose",
+        compiler_params=PARAMS,
+        cost_estimate=cost(main.size, main, helped),
+    )(main, helped)
 
 
 def is_inner():
@@ -519,18 +657,18 @@
     )(*mixed, *weights)
 
 
-def pair_kernel(kept_ref, came_ref, own_ref, *send_refs):
-    share = own_ref.shape[0]
-    for k, ref in enumerate((own_ref, *send_refs)):
-        rows = slice(k * share, (k + 1) * share)
+def pair_kernel(first, kept_ref, came_ref, *out_refs):
+    share = out_refs[0].shape[0]
+    for k, ref in enumerate(out_refs):
+        rows = slice((first + k) * share, (first + k + 1) * share)
         ref[...] = (kept_ref[rows, :] + came_ref[rows, :].astype(f32)).astype(ref.dtype)
 
 
-def pair_sum(kept, came):
+def pair_sum(kept, came, first, count, dtype):
     share = (kept.shape[0] // 4, kept.shape[1])
-    outs = (jax.ShapeDtypeStruct(share, f32),) + (jax.ShapeDtypeStruct(share, bf16),) * 3
+    outs = (jax.ShapeDtypeStruct(share, dtype),) * count
     return pl.pallas_call(
-        pair_kernel,
+        functools.partial(pair_kernel, first),
         out_shape=outs,
         name="pair",
         compiler_params=PARAMS,
@@ -575,40 +713,21 @@
     )(*arrays)
 
 
-def fast_shards(
-    sizes,
-    recurrent_query,
-    recurrent_forget_gate,
-    recurrent_value,
-    recurrent_gate_lower_bound,
-    recurrent_added_decay,
-    recurrent_norm_gain,
-    attention_query_first,
-    attention_key_first,
-    attention_query_second,
-    attention_key_second,
-    attention_value,
-    second_map_weight,
-    attention_norm_gain,
-    output_weight,
-):
+def fast_shards(sizes, *arrays):
     grp_size, sp_size, tp_size = sizes
+    output_weight = arrays[13]
+    tokens = arrays[0].shape[0]
 
     def swap(array, axis, size, d):
         return lax.ppermute(array, axis, [(k, k ^ d) for k in range(size)])
 
-    def up(array, first):
-        return lax.ppermute(array, "sp", [(k, k + 1) for k in range(first, sp_size - 1)])
-
     last = sp_size - 1
-    inner = [(k, last - k) for k in range(1, last)]
-    outward = [(1, 0), (last - 1, last)]
-    own_keys = jnp.concatenate(
-        [attention_key_first, attention_key_second, attention_value], axis=1
-    )
-    key_hops = [own_keys]
-    for k in range(last):
-        key_hops.append(up(key_hops[-1], k))
+    inner = [(1, 2), (2, 1)]
+    outward = [(1, 0), (2, last)]
+    local, faded, packed, front, asked, gains, weight = prepare(last, arrays[:13])
+    p1 = lax.ppermute(front, "sp", [(0, 1), (last, 2)])
+    p2 = lax.ppermute(packed, "sp", [(1, 2)])
+    p3 = lax.ppermute(packed, "sp", [(0, 2)])
     half = output_weight.shape[2] // grp_size
     own_weight = lax.dynamic_slice_in_dim(
         output_weight, lax.axis_index("grp") * half, half, axis=2
@@ -618,25 +737,12 @@
     weight_mid_far = lax.ppermute(weight_one, "sp", inner)
     weight_end = lax.ppermute(weight_mid, "sp", outward)
     weight_end_far = lax.ppermute(weight_mid_far, "sp", outward)
-    local, faded, state = local_recurrence(
-        recurrent_query,
-        recurrent_forget_gate,
-        recurrent_value,
-        recurrent_gate_lower_bound,
-        recurrent_added_decay,
-    )
-    below = up(state, 0)
-    two = merge_states(state, below)
-    far = lax.ppermute(two, "sp", [(k, k + 2) for k in range(sp_size - 2)])
-    attended = attention(
-        attention_query_first,
-        attention_query_second,
-        own_keys,
-        key_hops[1:],
-        second_map_weight,
-        attention_norm_gain,
-    )
-    recurrent = carry_in(local, faded, recurrent_norm_gain, (below, far))
+    p4 = lax.ppermute(blend(packed, p2, p3), "sp", [(2, last)])
+    helped = attention(helper_kernel, last, tokens, packed, p1, p2, p3, weight, gains)
+    p5 = lax.ppermute(helped, "sp", [(2, last)])
+    main = attention(main_kernel, last, tokens, asked, packed, p1, p2, p3, weight, gains)
+    recurrent = carry_in(local, faded, gains, p1, p2, p3, p4)
+    attended = choose(last, main, p5)
     mixed = (
         recurrent, attended, swap(recurrent, "grp", grp_size, 1), swap(attended, "grp", grp_size, 1)
     )
@@ -654,7 +760,8 @@
         sent = project(1, tp_size, mixed, weights, bf16)
         came = swap(sent, "tp", tp_size, 1)
         kept = project(0, tp_size, mixed, weights, f32)
-        own, across, beside, corner = pair_sum(kept, came)
+        across, beside, corner = pair_sum(kept, came, 1, 3, bf16)
+        (own,) = pair_sum(kept, came, 0, 1, f32)
         across = swap(across, "tp", tp_size, 2)
         beside = swap(beside, "grp", grp_size, 1)
         corner = lax.ppermute(corner, ("grp", "tp"), corner_pairs)

time: 68 us -> 69 us (1.015)
  the two profiles are of different devices: /device:TPU:0 before, /device:TPU:24 now
where the time goes in v1:
time: 69 us; the launch traced here: 68.8 us
  waiting for transfers between devices  39.9 us (58%)
  starting transfers between devices  23.7 us (34%)
  Pallas kernels  4.93 us (7%)
    ppermute x1, waiting for transfers between devices, fast_shards(): p4 = lax.ppermute(blend(packed, p2, p3), 'sp', [(2, last)])  17.9 us
    ppermute x9, starting transfers between devices, swap(): return lax.ppermute(array, axis, [(k, k ^ d) for k in range(size)])  10.8 us
    ppermute x1, waiting for transfers between devices, fast_shards(): weight_end_far = lax.ppermute(weight_mid_far, 'sp', outward)  9.28 us
    ppermute x9, waiting for transfers between devices, swap(): return lax.ppermute(array, axis, [(k, k ^ d) for k in range(size)])  7.87 us
    ppermute x2, starting transfers between devices, fast_shards(): corner = lax.ppermute(corner, ('grp', 'tp'), corner_pairs)  2.64 us
    ppermute x2, waiting for transfers between devices, fast_shards(): corner = lax.ppermute(corner, ('grp', 'tp'), corner_pairs)  2.61 us
    pallas_call x1, Pallas kernels, prepare(): pl.pallas_call(functools.partial(prepare_kernel, last), out_shape=outs, i...  2.46 us
    ppermute x1, starting transfers between devices, fast_shards(): p1 = lax.ppermute(front, 'sp', [(0, 1), (last, 2)])  2.37 us
  transfers between devices with their start and end apart: 20, of which 8 were waited for; matrix products, arithmetic and copies ran while one was open for 0% of the time, Pallas kernels for 2%

profile of v1, /device:TPU:24, one launch (start us, length us, event | category | flops | bytes accessed | tf_op | source)
XLA Modules:
  0.0 68.8 jit_solution(13041147084474359716)
XLA Ops:
  0.0 2.5 %prepare.1 = (f32[256,256]{1,0:T(8,128)S(1)}, bf16[256,256]{1,0:T(8,128)(2,1)S(1)}, bf16[400,256]{1,0:T(8,128)(2,1)S(1)}, bf16[512,256]{1,0:T(8,128)(2,1)S(1)}, ...) custom-call(bf16[64,256]{1,0:T(8,128)(2,1)} %bitcast.7, bf16[64,256]{1,0:T(8,128)(2,1)} %bitcast.8, ...), custom_call_target="tpu_custom_call" | custom-call | flops 134217728 | bytes 1385480 | tf_op jit(solution)/shard_map/prepare/pallas_call | solution.py:454
  2.5 2.4 %collective-permute-start = (bf16[512,256]{1,0:T(8,128)(2,1)S(1)}, bf16[512,256]{1,0:T(8,128)(2,1)S(1)}, u32[]{:S(2)}, u32[]{:S(2)}) collective-permute-start(bf16[512,256]{1,0:T(8,128)(2,1)S(1)} %get-tuple-element.21), channel_id=1, source_target_pairs={{0,4},{12,8},{1,5},{13,9},{2,6},{14,10},{3,7},{15,11},{16,20},{28,... | collective-permute-start | bytes 786440 | tf_op jit(solution)/shard_map/ppermute | solution.py:728
  4.9 0.7 collective-permute-start.8
  5.6 0.7 collective-permute-start.1
  6.9 2.4 %collective-permute-start.7 = (bf16[2,256,256]{2,1,0:T(8,128)(2,1)S(1)}, bf16[2,256,256]{2,1,0:T(8,128)(2,1)S(1)}, u32[]{:S(2)}, u32[]{:S(2)}) collective-permute-start(bf16[2,256,256]{2,1,0:T(8,128)(2,1)S(1)} %constant_dynamic-slice_fusion.refs_4_), channel_id=1, source_target_pairs={{0,4},{4,0},{8,12},{12,8},{1,5},{5,1},{9,13},{13,9},{2,6},{6,2},{1... | collective-permute-start | bytes 786440 | tf_op jit(solution)/shard_map/ppermute | solution.py:722
  9.3 2.2 %collective-permute-done.p1_ref = bf16[512,256]{1,0:T(8,128)(2,1)S(1)} collective-permute-done((bf16[512,256]{1,0:T(8,128)(2,1)S(1)}, bf16[512,256]{1,0:T(8,128)(2,1)S(1)}, u32[]{:S(2)}, u32[]{:S(2)}) %collective-permute-start) | collective-permute-done | bytes 262176 | tf_op jit(solution)/shard_map/ppermute | solution.py:728
  11.5 1.3 %collective-permute-start.4 = (bf16[256,256]{1,0:T(8,128)(2,1)S(1)}, bf16[256,256]{1,0:T(8,128)(2,1)S(1)}, u32[]{:S(2)}, u32[]{:S(2)}) collective-permute-start(bf16[256,256]{1,0:T(8,128)(2,1)S(1)} %shard_map.137), channel_id=1, source_target_pairs={{8,12},{9,13},{10,14},{11,15},{24,28},{25,29},{26,30},{27,31}} | collective-permute-start | bytes 393224 | tf_op jit(solution)/shard_map/ppermute | solution.py:742
  12.8 1.3 %collective-permute-start.9 = (bf16[2,256,256]{2,1,0:T(8,128)(2,1)S(1)}, bf16[2,256,256]{2,1,0:T(8,128)(2,1)S(1)}, u32[]{:S(2)}, u32[]{:S(2)}) collective-permute-start(bf16[2,256,256]{2,1,0:T(8,128)(2,1)S(1)} %collective-permute-done.8.refs_7_), channel_id=1, source_target_pairs={{4,0},{8,12},{5,1},{9,13},{6,2},{10,14},{7,3},{11,15},{20,16},{24,... | collective-permute-start | bytes 786440 | tf_op jit(solution)/shard_map/ppermute | solution.py:738
  14.1 1.9 %collective-permute-done.7.refs_5_ = bf16[2,256,256]{2,1,0:T(8,128)(2,1)S(1)} collective-permute-done((bf16[2,256,256]{2,1,0:T(8,128)(2,1)S(1)}, bf16[2,256,256]{2,1,0:T(8,128)(2,1)S(1)}, u32[]{:S(2)}, u32[]{:S(2)}) %collective-permute-start.7) | collective-permute-done | bytes 262176 | tf_op jit(solution)/shard_map/ppermute | solution.py:722
  16.7 1.3 %collective-permute-start.3 = (bf16[128,256]{1,0:T(8,128)(2,1)S(1)}, bf16[128,256]{1,0:T(8,128)(2,1)S(1)}, u32[]{:S(2)}, u32[]{:S(2)}) collective-permute-start(bf16[128,256]{1,0:T(8,128)(2,1)S(1)} %blend.1), channel_id=1, source_target_pairs={{8,12},{9,13},{10,14},{11,15},{24,28},{25,29},{26,30},{27,31}} | collective-permute-start | bytes 196616 | tf_op jit(solution)/shard_map/ppermute | solution.py:740
  18.0 17.9 %collective-permute-done.3.p4_ref = bf16[128,256]{1,0:T(8,128)(2,1)S(1)} collective-permute-done((bf16[128,256]{1,0:T(8,128)(2,1)S(1)}, bf16[128,256]{1,0:T(8,128)(2,1)S(1)}, u32[]{:S(2)}, u32[]{:S(2)}) %collective-permute-start.3) | collective-permute-done | bytes 65568 | tf_op jit(solution)/shard_map/ppermute | solution.py:740
  36.3 1.6 %collective-permute-start.5 = (bf16[256,256]{1,0:T(8,128)(2,1)S(1)}, bf16[256,256]{1,0:T(8,128)(2,1)S(1)}, u32[]{:S(2)}, u32[]{:S(2)}) collective-permute-start(bf16[256,256]{1,0:T(8,128)(2,1)S(1)} %carry.1.refs_0_), channel_id=1, source_target_pairs={{0,16},{16,0},{1,17},{17,1},{2,18},{18,2},{3,19},{19,3},{4,20},{20... | collective-permute-start | bytes 393224 | tf_op jit(solution)/shard_map/ppermute | solution.py:722
  38.5 3.1 %collective-permute-done.5.refs_2_ = bf16[256,256]{1,0:T(8,128)(2,1)S(1)} collective-permute-done((bf16[256,256]{1,0:T(8,128)(2,1)S(1)}, bf16[256,256]{1,0:T(8,128)(2,1)S(1)}, u32[]{:S(2)}, u32[]{:S(2)}) %collective-permute-start.5) | collective-permute-done | bytes 131104 | tf_op jit(solution)/shard_map/ppermute | solution.py:722
  41.5 1.4 %collective-permute-done.6.refs_3_ = bf16[256,256]{1,0:T(8,128)(2,1)S(1)} collective-permute-done((bf16[256,256]{1,0:T(8,128)(2,1)S(1)}, bf16[256,256]{1,0:T(8,128)(2,1)S(1)}, u32[]{:S(2)}, u32[]{:S(2)}) %collective-permute-start.6) | collective-permute-done | bytes 131104 | tf_op jit(solution)/shard_map/ppermute | solution.py:722
  43.4 1.3 %collective-permute-start.15 = (bf16[2,256,256]{2,1,0:T(8,128)(2,1)S(1)}, bf16[2,256,256]{2,1,0:T(8,128)(2,1)S(1)}, u32[]{:S(2)}, u32[]{:S(2)}) collective-permute-start(bf16[2,256,256]{2,1,0:T(8,128)(2,1)S(1)} %collective-permute-done.14.refs_5_), channel_id=1, source_target_pairs={{4,0},{8,12},{5,1},{9,13},{6,2},{10,14},{7,3},{11,15},{20,16},{24,... | collective-permute-start | bytes 786440 | tf_op jit(solution)/shard_map/ppermute | solution.py:739
  44.7 9.3 %collective-permute-done.15.refs_4_ = bf16[2,256,256]{2,1,0:T(8,128)(2,1)S(1)} collective-permute-done((bf16[2,256,256]{2,1,0:T(8,128)(2,1)S(1)}, bf16[2,256,256]{2,1,0:T(8,128)(2,1)S(1)}, u32[]{:S(2)}, u32[]{:S(2)}) %collective-permute-start.15) | collective-permute-done | bytes 262176 | tf_op jit(solution)/shard_map/ppermute | solution.py:739
  54.8 1.6 %collective-permute-start.11 = (bf16[64,768]{1,0:T(8,128)(2,1)S(1)}, bf16[64,768]{1,0:T(8,128)(2,1)S(1)}, u32[]{:S(2)}, u32[]{:S(2)}) collective-permute-start(bf16[64,768]{1,0:T(8,128)(2,1)S(1)} %get-tuple-element.25), channel_id=1, source_target_pairs={{0,2},{1,3},{2,0},{3,1},{4,6},{5,7},{6,4},{7,5},{8,10},{9,11},{10,... | collective-permute-start | bytes 294920 | tf_op jit(solution)/shard_map/ppermute | solution.py:722
  56.3 1.5 %collective-permute-start.12 = (bf16[64,768]{1,0:T(8,128)(2,1)S(1)}, bf16[64,768]{1,0:T(8,128)(2,1)S(1)}, u32[]{:S(2)}, u32[]{:S(2)}) collective-permute-start(bf16[64,768]{1,0:T(8,128)(2,1)S(1)} %get-tuple-element.26), channel_id=1, source_target_pairs={{0,16},{16,0},{1,17},{17,1},{2,18},{18,2},{3,19},{19,3},{4,20},{20... | collective-permute-start | bytes 294920 | tf_op jit(solution)/shard_map/ppermute | solution.py:722
  58.6 1.6 %collective-permute-start.17 = (bf16[64,256]{1,0:T(8,128)(2,1)S(1)}, bf16[64,256]{1,0:T(8,128)(2,1)S(1)}, u32[]{:S(2)}, u32[]{:S(2)}) collective-permute-start(bf16[64,256]{1,0:T(8,128)(2,1)S(1)} %get-tuple-element.28), channel_id=1, source_target_pairs={{0,2},{1,3},{2,0},{3,1},{4,6},{5,7},{6,4},{7,5},{8,10},{9,11},{10,... | collective-permute-start | bytes 98312 | tf_op jit(solution)/shard_map/ppermute | solution.py:722
  60.2 1.5 %collective-permute-start.18 = (bf16[64,256]{1,0:T(8,128)(2,1)S(1)}, bf16[64,256]{1,0:T(8,128)(2,1)S(1)}, u32[]{:S(2)}, u32[]{:S(2)}) collective-permute-start(bf16[64,256]{1,0:T(8,128)(2,1)S(1)} %get-tuple-element.29), channel_id=1, source_target_pairs={{0,16},{16,0},{1,17},{17,1},{2,18},{18,2},{3,19},{19,3},{4,20},{20... | collective-permute-start | bytes 98312 | tf_op jit(solution)/shard_map/ppermute | solution.py:722
  61.7 1.5 %collective-permute-done.17.refs_5_ = bf16[64,256]{1,0:T(8,128)(2,1)S(1)} collective-permute-done((bf16[64,256]{1,0:T(8,128)(2,1)S(1)}, bf16[64,256]{1,0:T(8,128)(2,1)S(1)}, u32[]{:S(2)}, u32[]{:S(2)}) %collective-permute-start.17) | collective-permute-done | bytes 32800 | tf_op jit(solution)/shard_map/ppermute | solution.py:722
  63.2 2.2 %collective-permute-start.19 = (bf16[64,256]{1,0:T(8,128)(2,1)S(1)}, bf16[64,256]{1,0:T(8,128)(2,1)S(1)}, u32[]{:S(2)}, u32[]{:S(2)}) collective-permute-start(bf16[64,256]{1,0:T(8,128)(2,1)S(1)} %get-tuple-element.30), channel_id=1, source_target_pairs={{0,18},{1,19},{2,16},{3,17},{16,2},{17,3},{18,0},{19,1},{4,22},{5,... | collective-permute-start | bytes 98312 | tf_op jit(solution)/shard_map/ppermute | solution.py:767
  65.4 2.6 %collective-permute-done.19.refs_7_ = bf16[64,256]{1,0:T(8,128)(2,1)S(1)} collective-permute-done((bf16[64,256]{1,0:T(8,128)(2,1)S(1)}, bf16[64,256]{1,0:T(8,128)(2,1)S(1)}, u32[]{:S(2)}, u32[]{:S(2)}) %collective-permute-start.19) | collective-permute-done | bytes 32800 | tf_op jit(solution)/shard_map/ppermute | solution.py:767
  68.0 0.8 %final.1 = bf16[64,2048]{1,0:T(8,128)(2,1)} custom-call(f32[64,768]{1,0:T(8,128)S(1)} %pair.4.refs_0_, bf16[64,768]{1,0:T(8,128)(2,1)S(1)} %collective-permute-done.11.refs_1_, bf16[64,768]{1,0:T(8,128)(2,1)S(1)} %collective-permute-done.12.refs_2_, bf16[64,768]{1,0:T(8,128)(2,1)S(1)} %collective-permute-done.13.refs_3_, f32[64,256]{1,0:T(8,128)S(1)} %pair.6.refs_4_, ...), custom_call_target="tpu_custom_call" | custom-call | flops 131072 | bytes 917504 | tf_op jit(solution)/shard_map/final/pallas_call | solution.py:707
  (34 shorter events, 4.3 us)
Async XLA Ops:
  0.0 4.9 %copy-start = (bf16[2,256,512]{2,1,0:T(8,128)(2,1)S(1)}, bf16[2,256,512]{2,1,0:T(8,128)(2,1)}, u32[]{:S(2)}) copy-start(bf16[2,256,512]{2,1,0:T(8,128)(2,1)} %param.27) | copy-start | bytes 1572868
  2.5 9.0 %collective-permute-start = (bf16[512,256]{1,0:T(8,128)(2,1)S(1)}, bf16[512,256]{1,0:T(8,128)(2,1)S(1)}, u32[]{:S(2)}, u32[]{:S(2)}) collective-permute-start(bf16[512,256]{1,0:T(8,128)(2,1)S(1)} %get-tuple-element.21), channel_id=1, source_target_pairs={{0,4},{12,8},{1,5},{13,9},{2,6},{14,10},{3,7},{15,11},{16,20},{28,... | collective-permute-start | bytes 786440 | tf_op jit(solution)/shard_map/ppermute | solution.py:728
  4.9 7.9 %collective-permute-start.8 = (bf16[2,256,256]{2,1,0:T(8,128)(2,1)S(1)}, bf16[2,256,256]{2,1,0:T(8,128)(2,1)S(1)}, u32[]{:S(2)}, u32[]{:S(2)}) collective-permute-start(bf16[2,256,256]{2,1,0:T(8,128)(2,1)S(1)} %constant_dynamic-slice_fusion.refs_4_), channel_id=1, source_target_pairs={{4,8},{8,4},{5,9},{9,5},{6,10},{10,6},{7,11},{11,7},{20,24},{24,20... | collective-permute-start | bytes 786440 | tf_op jit(solution)/shard_map/ppermute | solution.py:736
  5.6 3.7 %collective-permute-start.1 = (bf16[400,256]{1,0:T(8,128)(2,1)S(1)}, bf16[400,256]{1,0:T(8,128)(2,1)S(1)}, u32[]{:S(2)}, u32[]{:S(2)}) collective-permute-start(bf16[400,256]{1,0:T(8,128)(2,1)S(1)} %get-tuple-element.22.own_ref), channel_id=1, source_target_pairs={{4,8},{5,9},{6,10},{7,11},{20,24},{21,25},{22,26},{23,27}} | collective-permute-start | bytes 614408 | tf_op jit(solution)/shard_map/ppermute | solution.py:729
  6.3 3.0 %collective-permute-start.2 = (bf16[400,256]{1,0:T(8,128)(2,1)S(1)}, bf16[400,256]{1,0:T(8,128)(2,1)S(1)}, u32[]{:S(2)}, u32[]{:S(2)}) collective-permute-start(bf16[400,256]{1,0:T(8,128)(2,1)S(1)} %get-tuple-element.22.own_ref), channel_id=1, source_target_pairs={{0,8},{1,9},{2,10},{3,11},{16,24},{17,25},{18,26},{19,27}} | collective-permute-start | bytes 614408 | tf_op jit(solution)/shard_map/ppermute | solution.py:730
  6.9 9.1 %collective-permute-start.7 = (bf16[2,256,256]{2,1,0:T(8,128)(2,1)S(1)}, bf16[2,256,256]{2,1,0:T(8,128)(2,1)S(1)}, u32[]{:S(2)}, u32[]{:S(2)}) collective-permute-start(bf16[2,256,256]{2,1,0:T(8,128)(2,1)S(1)} %constant_dynamic-slice_fusion.refs_4_), channel_id=1, source_target_pairs={{0,4},{4,0},{8,12},{12,8},{1,5},{5,1},{9,13},{13,9},{2,6},{6,2},{1... | collective-permute-start | bytes 786440 | tf_op jit(solution)/shard_map/ppermute | solution.py:722
  11.5 26.4 %collective-permute-start.4 = (bf16[256,256]{1,0:T(8,128)(2,1)S(1)}, bf16[256,256]{1,0:T(8,128)(2,1)S(1)}, u32[]{:S(2)}, u32[]{:S(2)}) collective-permute-start(bf16[256,256]{1,0:T(8,128)(2,1)S(1)} %shard_map.137), channel_id=1, source_target_pairs={{8,12},{9,13},{10,14},{11,15},{24,28},{25,29},{26,30},{27,31}} | collective-permute-start | bytes 393224 | tf_op jit(solution)/shard_map/ppermute | solution.py:742
  12.8 30.1 %collective-permute-start.9 = (bf16[2,256,256]{2,1,0:T(8,128)(2,1)S(1)}, bf16[2,256,256]{2,1,0:T(8,128)(2,1)S(1)}, u32[]{:S(2)}, u32[]{:S(2)}) collective-permute-start(bf16[2,256,256]{2,1,0:T(8,128)(2,1)S(1)} %collective-permute-done.8.refs_7_), channel_id=1, source_target_pairs={{4,0},{8,12},{5,1},{9,13},{6,2},{10,14},{7,3},{11,15},{20,16},{24,... | collective-permute-start | bytes 786440 | tf_op jit(solution)/shard_map/ppermute | solution.py:738
  16.0 27.4 %collective-permute-start.14 = (bf16[2,256,256]{2,1,0:T(8,128)(2,1)S(1)}, bf16[2,256,256]{2,1,0:T(8,128)(2,1)S(1)}, u32[]{:S(2)}, u32[]{:S(2)}) collective-permute-start(bf16[2,256,256]{2,1,0:T(8,128)(2,1)S(1)} %collective-permute-done.7.refs_5_), channel_id=1, source_target_pairs={{4,8},{8,4},{5,9},{9,5},{6,10},{10,6},{7,11},{11,7},{20,24},{24,20... | collective-permute-start | bytes 786440 | tf_op jit(solution)/shard_map/ppermute | solution.py:737
  16.7 19.2 %collective-permute-start.3 = (bf16[128,256]{1,0:T(8,128)(2,1)S(1)}, bf16[128,256]{1,0:T(8,128)(2,1)S(1)}, u32[]{:S(2)}, u32[]{:S(2)}) collective-permute-start(bf16[128,256]{1,0:T(8,128)(2,1)S(1)} %blend.1), channel_id=1, source_target_pairs={{8,12},{9,13},{10,14},{11,15},{24,28},{25,29},{26,30},{27,31}} | collective-permute-start | bytes 196616 | tf_op jit(solution)/shard_map/ppermute | solution.py:740
  36.3 5.3 %collective-permute-start.5 = (bf16[256,256]{1,0:T(8,128)(2,1)S(1)}, bf16[256,256]{1,0:T(8,128)(2,1)S(1)}, u32[]{:S(2)}, u32[]{:S(2)}) collective-permute-start(bf16[256,256]{1,0:T(8,128)(2,1)S(1)} %carry.1.refs_0_), channel_id=1, source_target_pairs={{0,16},{16,0},{1,17},{17,1},{2,18},{18,2},{3,19},{19,3},{4,20},{20... | collective-permute-start | bytes 393224 | tf_op jit(solution)/shard_map/ppermute | solution.py:722
  37.9 5.1 %collective-permute-start.6 = (bf16[256,256]{1,0:T(8,128)(2,1)S(1)}, bf16[256,256]{1,0:T(8,128)(2,1)S(1)}, u32[]{:S(2)}, u32[]{:S(2)}) collective-permute-start(bf16[256,256]{1,0:T(8,128)(2,1)S(1)} %choose.1.refs_1_), channel_id=1, source_target_pairs={{0,16},{16,0},{1,17},{17,1},{2,18},{18,2},{3,19},{19,3},{4,20},{20... | collective-permute-start | bytes 393224 | tf_op jit(solution)/shard_map/ppermute | solution.py:722
  43.3 11.4 %collective-permute-start.10 = (bf16[256,768]{1,0:T(8,128)(2,1)S(1)}, bf16[256,768]{1,0:T(8,128)(2,1)S(1)}, u32[]{:S(2)}, u32[]{:S(2)}) collective-permute-start(bf16[256,768]{1,0:T(8,128)(2,1)S(1)} %project.5), channel_id=1, source_target_pairs={{0,1},{1,0},{2,3},{3,2},{4,5},{5,4},{6,7},{7,6},{8,9},{9,8},{10,11... | collective-permute-start | bytes 1179656 | tf_op jit(solution)/shard_map/ppermute | solution.py:722
  43.4 10.6 %collective-permute-start.15 = (bf16[2,256,256]{2,1,0:T(8,128)(2,1)S(1)}, bf16[2,256,256]{2,1,0:T(8,128)(2,1)S(1)}, u32[]{:S(2)}, u32[]{:S(2)}) collective-permute-start(bf16[2,256,256]{2,1,0:T(8,128)(2,1)S(1)} %collective-permute-done.14.refs_5_), channel_id=1, source_target_pairs={{4,0},{8,12},{5,1},{9,13},{6,2},{10,14},{7,3},{11,15},{20,16},{24,... | collective-permute-start | bytes 786440 | tf_op jit(solution)/shard_map/ppermute | solution.py:739
  54.2 4.3 %collective-permute-start.16 = (bf16[256,256]{1,0:T(8,128)(2,1)S(1)}, bf16[256,256]{1,0:T(8,128)(2,1)S(1)}, u32[]{:S(2)}, u32[]{:S(2)}) collective-permute-start(bf16[256,256]{1,0:T(8,128)(2,1)S(1)} %project.7), channel_id=1, source_target_pairs={{0,1},{1,0},{2,3},{3,2},{4,5},{5,4},{6,7},{7,6},{8,9},{9,8},{10,11... | collective-permute-start | bytes 393224 | tf_op jit(solution)/shard_map/ppermute | solution.py:722
  54.8 13.2 %collective-permute-start.11 = (bf16[64,768]{1,0:T(8,128)(2,1)S(1)}, bf16[64,768]{1,0:T(8,128)(2,1)S(1)}, u32[]{:S(2)}, u32[]{:S(2)}) collective-permute-start(bf16[64,768]{1,0:T(8,128)(2,1)S(1)} %get-tuple-element.25), channel_id=1, source_target_pairs={{0,2},{1,3},{2,0},{3,1},{4,6},{5,7},{6,4},{7,5},{8,10},{9,11},{10,... | collective-permute-start | bytes 294920 | tf_op jit(solution)/shard_map/ppermute | solution.py:722
  56.3 11.7 %collective-permute-start.12 = (bf16[64,768]{1,0:T(8,128)(2,1)S(1)}, bf16[64,768]{1,0:T(8,128)(2,1)S(1)}, u32[]{:S(2)}, u32[]{:S(2)}) collective-permute-start(bf16[64,768]{1,0:T(8,128)(2,1)S(1)} %get-tuple-element.26), channel_id=1, source_target_pairs={{0,16},{16,0},{1,17},{17,1},{2,18},{18,2},{3,19},{19,3},{4,20},{20... | collective-permute-start | bytes 294920 | tf_op jit(solution)/shard_map/ppermute | solution.py:722
  57.8 10.1 %collective-permute-start.13 = (bf16[64,768]{1,0:T(8,128)(2,1)S(1)}, bf16[64,768]{1,0:T(8,128)(2,1)S(1)}, u32[]{:S(2)}, u32[]{:S(2)}) collective-permute-start(bf16[64,768]{1,0:T(8,128)(2,1)S(1)} %get-tuple-element.27), channel_id=1, source_target_pairs={{0,18},{1,19},{2,16},{3,17},{16,2},{17,3},{18,0},{19,1},{4,22},{5,... | collective-permute-start | bytes 294920 | tf_op jit(solution)/shard_map/ppermute | solution.py:767
  58.6 4.6 %collective-permute-start.17 = (bf16[64,256]{1,0:T(8,128)(2,1)S(1)}, bf16[64,256]{1,0:T(8,128)(2,1)S(1)}, u32[]{:S(2)}, u32[]{:S(2)}) collective-permute-start(bf16[64,256]{1,0:T(8,128)(2,1)S(1)} %get-tuple-element.28), channel_id=1, source_target_pairs={{0,2},{1,3},{2,0},{3,1},{4,6},{5,7},{6,4},{7,5},{8,10},{9,11},{10,... | collective-permute-start | bytes 98312 | tf_op jit(solution)/shard_map/ppermute | solution.py:722
  60.2 5.2 %collective-permute-start.18 = (bf16[64,256]{1,0:T(8,128)(2,1)S(1)}, bf16[64,256]{1,0:T(8,128)(2,1)S(1)}, u32[]{:S(2)}, u32[]{:S(2)}) collective-permute-start(bf16[64,256]{1,0:T(8,128)(2,1)S(1)} %get-tuple-element.29), channel_id=1, source_target_pairs={{0,16},{16,0},{1,17},{17,1},{2,18},{18,2},{3,19},{19,3},{4,20},{20... | collective-permute-start | bytes 98312 | tf_op jit(solution)/shard_map/ppermute | solution.py:722
  63.2 4.8 %collective-permute-start.19 = (bf16[64,256]{1,0:T(8,128)(2,1)S(1)}, bf16[64,256]{1,0:T(8,128)(2,1)S(1)}, u32[]{:S(2)}, u32[]{:S(2)}) collective-permute-start(bf16[64,256]{1,0:T(8,128)(2,1)S(1)} %get-tuple-element.30), channel_id=1, source_target_pairs={{0,18},{1,19},{2,16},{3,17},{16,2},{17,3},{18,0},{19,1},{4,22},{5,... | collective-permute-start | bytes 98312 | tf_op jit(solution)/shard_map/ppermute | solution.py:767

commit v2 on v1

--- a/solution.py
+++ b/solution.py
@@ -309,7 +309,7 @@
 VMEM = pl.BlockSpec(memory_space=pltpu.VMEM)
 
 
-def prepare_kernel(last, *refs):
+def prepare_kernel(*refs):
     sources, rest = refs[:13], refs[13:]
     local_ref, faded_ref, packed_ref, front_ref, asked_ref, gain_ref, weight_ref = rest[:7]
     query_ref, gate_ref, value_ref, bound_ref, added_ref, lift_ref, sems = rest[7:]
@@ -336,9 +336,9 @@
         pltpu.make_async_copy(source, target, sems.at[k])
         for k, (source, target) in enumerate(zip(sources, targets))
     ]
-    for copy in copies:
+    for copy in copies[5:] + copies[:5]:
         copy.start()
-    for copy in copies[5:]:
+    for copy in copies[5:8]:
         copy.wait()
     floor_rate = jax.nn.sigmoid(-bound_ref[...])
     inflow = floor_rate * jax.nn.sigmoid(-gate_ref[...].astype(f32))
@@ -349,6 +349,8 @@
     lower = jnp.where(causal, 1.0, 0.0).astype(bf16)
     total = jnp.zeros((1, width), f32)
     states = [None] * heads
+    for copy in copies[8:]:
+        copy.wait()
     for n in range(token_count // chunk):
         rows = slice(n * chunk, (n + 1) * chunk)
         steps = log_decay[rows]
@@ -396,18 +398,10 @@
         block = lift_ref[n * wide : (n + 1) * wide, :]
         packed_ref[wide:BASE, n * wide : (n + 1) * wide] = block
     front_ref[:BASE, :] = packed_ref[:BASE, :]
-    at_end = lax.axis_index("sp") == last
-
-    @pl.when(at_end)
-    def _():
-        front_ref[BASE:, :] = asked_ref[...]
-
-    @pl.when(jnp.logical_not(at_end))
-    def _():
-        front_ref[BASE : BASE + HG_DV + SPARE_ROWS, :] = packed_ref[BASE:, :]
-
-
-def prepare(last, arrays):
+    front_ref[BASE:, :] = asked_ref[...]
+
+
+def prepare(arrays):
     (
         query,
         gate,
@@ -452,7 +446,7 @@
         weight.reshape(1, -1),
     )
     return pl.pallas_call(
-        functools.partial(prepare_kernel, last),
+        prepare_kernel,
         out_shape=outs,
         in_specs=[HBM] * len(inputs),
         out_specs=[VMEM] * len(outs),
@@ -594,62 +588,44 @@
     )(*arrays)
 
 
-def choose_kernel(last, main_ref, helped_ref, out_ref):
-    at_end = lax.axis_index("sp") == last
-
-    @pl.when(at_end)
-    def _():
-        out_ref[...] = helped_ref[...]
-
-    @pl.when(jnp.logical_not(at_end))
-    def _():
-        out_ref[...] = main_ref[...]
-
-
-def choose(last, main, helped):
-    return pl.pallas_call(
-        functools.partial(choose_kernel, last),
-        out_shape=jax.ShapeDtypeStruct(main.shape, bf16),
-        name="choose",
-        compiler_params=PARAMS,
-        cost_estimate=cost(main.size, main, helped),
-    )(main, helped)
-
-
-def is_inner():
-    place = lax.axis_index("sp")
-    return jnp.logical_and(place > 0, place < lax.axis_size("sp") - 1)
-
-
-def project_kernel(flip, tp_size, counts, *refs):
-    mixed_refs, weight_refs, out_ref = refs[:4], list(refs[4:-1]), refs[-1]
-    share = mixed_refs[0].shape[0] // tp_size
+def project_kernel(flip, tp_size, last, counts, *refs):
+    recurrent_refs, main_refs, helped_refs = refs[0:2], refs[2:4], refs[4:6]
+    weight_refs, out_ref = list(refs[6:-1]), refs[-1]
+    share = recurrent_refs[0].shape[0] // tp_size
     place = lax.axis_index("tp")
-
-    def rows_of(ref):
-        return [
-            ref[pl.ds(pl.multiple_of((place ^ flip ^ across) * share, share), share), :]
-            for across in (0, 2)
-        ]
-
-    recurrent = jnp.concatenate(rows_of(mixed_refs[0]) + rows_of(mixed_refs[2]), axis=0)
-    attended = jnp.concatenate(rows_of(mixed_refs[1]) + rows_of(mixed_refs[3]), axis=0)
+    at = lax.axis_index("sp")
+    at_end = at == last
+    inner = jnp.logical_and(at > 0, at < last)
+
+    def rows_of(pair):
+        return jnp.concatenate(
+            [
+                ref[pl.ds(pl.multiple_of((place ^ flip ^ across) * share, share), share), :]
+                for ref in pair
+                for across in (0, 2)
+            ],
+            axis=0,
+        )
+
+    recurrent = rows_of(recurrent_refs)
+    attended = jnp.where(at_end, rows_of(helped_refs), rows_of(main_refs))
     for p, count in enumerate(counts):
         weight = weight_refs.pop(0)[...]
         if count == 2:
-            weight = jnp.where(is_inner(), weight_refs.pop(0)[...], weight)
+            weight = jnp.where(inner, weight_refs.pop(0)[...], weight)
         width = weight.shape[2]
         terms = dot_nn(recurrent, weight[0]) + dot_nn(attended, weight[1])
         out_ref[:, p * width : (p + 1) * width] = terms.astype(out_ref.dtype)
 
 
-def project(flip, tp_size, mixed, weights, dtype):
+def project(flip, sizes, mixed, weights, dtype):
+    _, sp_size, tp_size = sizes
     rows = 4 * (mixed[0].shape[0] // tp_size)
     counts = tuple(len(w) for w in weights)
     weights = [w for choice in weights for w in choice]
     out = jax.ShapeDtypeStruct((rows, weights[0].shape[2] * len(counts)), dtype)
     return pl.pallas_call(
-        functools.partial(project_kernel, flip, tp_size, counts),
+        functools.partial(project_kernel, flip, tp_size, sp_size - 1, counts),
         out_shape=out,
         name="project",
         compiler_params=PARAMS,
@@ -676,20 +652,16 @@
     )(kept, came)
 
 
-def final_kernel(counts, *refs):
+def final_kernel(*refs):
     out_ref = refs[-1]
     group = lax.axis_index("grp")
     place = lax.axis_index("sp")
-    turn = jnp.where(is_inner(), 1, 0)
-    piece = 0
-    for n, count in enumerate(counts):
+    for n, pieces in enumerate(GROUPS):
         own_ref, across_ref, beside_ref, corner_ref = refs[4 * n : 4 * n + 4]
-        width = own_ref.shape[1] // count
-        for p in range(count):
+        width = own_ref.shape[1] // len(pieces)
+        for p, d in enumerate(pieces):
             lanes = slice(p * width, (p + 1) * width)
-            shard = place ^ piece if piece < 2 else place ^ piece ^ turn
-            piece += 1
-            start = shard * (2 * width)
+            start = (place ^ d) * (2 * width)
             mine = own_ref[:, lanes] + across_ref[:, lanes].astype(f32)
             theirs = beside_ref[:, lanes].astype(f32) + corner_ref[:, lanes].astype(f32)
             first = pl.multiple_of(start + group * width, width)
@@ -698,14 +670,13 @@
             out_ref[:, pl.ds(second, width)] = theirs.astype(bf16)
 
 
-def final_sum(pieces, results):
+def final_sum(results):
     arrays = [array for result in results for array in result]
     rows = arrays[0].shape[0]
     width = sum(result[0].shape[1] for result in results)
-    counts = tuple(pieces * result[0].shape[1] // width for result in results)
     out = jax.ShapeDtypeStruct((rows, 2 * width), bf16)
     return pl.pallas_call(
-        functools.partial(final_kernel, counts),
+        final_kernel,
         out_shape=out,
         name="final",
         compiler_params=PARAMS,
@@ -722,10 +693,9 @@
         return lax.ppermute(array, axis, [(k, k ^ d) for k in range(size)])
 
     last = sp_size - 1
-    inner = [(1, 2), (2, 1)]
-    outward = [(1, 0), (2, last)]
-    local, faded, packed, front, asked, gains, weight = prepare(last, arrays[:13])
-    p1 = lax.ppermute(front, "sp", [(0, 1), (last, 2)])
+    local, faded, packed, front, asked, gains, weight = prepare(arrays[:13])
+    p0 = lax.ppermute(front, "sp", [(last, 2)])
+    p1 = lax.ppermute(packed, "sp", [(0, 1)])
     p2 = lax.ppermute(packed, "sp", [(1, 2)])
     p3 = lax.ppermute(packed, "sp", [(0, 2)])
     half = output_weight.shape[2] // grp_size
@@ -733,40 +703,57 @@
         output_weight, lax.axis_index("grp") * half, half, axis=2
     )
     weight_one = swap(own_weight, "sp", sp_size, 1)
-    weight_mid = lax.ppermute(own_weight, "sp", inner)
-    weight_mid_far = lax.ppermute(weight_one, "sp", inner)
-    weight_end = lax.ppermute(weight_mid, "sp", outward)
-    weight_end_far = lax.ppermute(weight_mid_far, "sp", outward)
+    weight_mid = lax.ppermute(own_weight, "sp", [(1, 2), (2, 1)])
+    weight_far = lax.ppermute(own_weight, "sp", [(0, last), (last, 0)])
+    weight_two = lax.ppermute(own_weight, "sp", [(0, 2), (last, 1)])
+    weight_end = lax.ppermute(weight_mid, "sp", [(1, 0), (2, last)])
     p4 = lax.ppermute(blend(packed, p2, p3), "sp", [(2, last)])
-    helped = attention(helper_kernel, last, tokens, packed, p1, p2, p3, weight, gains)
+    helped = attention(helper_kernel, last, tokens, packed, p0, p2, p3, weight, gains)
+    helped, asked = lax.optimization_barrier((helped, asked))
     p5 = lax.ppermute(helped, "sp", [(2, last)])
     main = attention(main_kernel, last, tokens, asked, packed, p1, p2, p3, weight, gains)
     recurrent = carry_in(local, faded, gains, p1, p2, p3, p4)
-    attended = choose(last, main, p5)
+    ends = [
+        (g * sp_size + last - 1, (g ^ 1) * sp_size + last) for g in range(grp_size)
+    ]
+    others = [
+        (g * sp_size + k, (g ^ 1) * sp_size + k) for g in range(grp_size) for k in range(last)
+    ]
     mixed = (
-        recurrent, attended, swap(recurrent, "grp", grp_size, 1), swap(attended, "grp", grp_size, 1)
+        recurrent,
+        swap(recurrent, "grp", grp_size, 1),
+        main,
+        lax.ppermute(main, ("grp", "sp"), others),
+        p5,
+        lax.ppermute(helped, ("grp", "sp"), ends),
     )
     corner_pairs = [
         (g * tp_size + k, (g ^ 1) * tp_size + (k ^ 2))
         for g in range(grp_size)
         for k in range(tp_size)
     ]
-    groups = (
-        ((own_weight,), (weight_one,), (weight_end, weight_mid)),
-        ((weight_end_far, weight_mid_far),),
-    )
+    weights = (
+        (own_weight,),
+        (weight_one,),
+        (weight_end, weight_two),
+        (weight_far, weight_mid),
+    )
+    groups = [[weights[d] for d in group] for group in GROUPS]
     results = []
     for weights in groups:
-        sent = project(1, tp_size, mixed, weights, bf16)
+        sent = project(1, sizes, mixed, weights, bf16)
         came = swap(sent, "tp", tp_size, 1)
-        kept = project(0, tp_size, mixed, weights, f32)
+        kept = project(0, sizes, mixed, weights, f32)
         across, beside, corner = pair_sum(kept, came, 1, 3, bf16)
         (own,) = pair_sum(kept, came, 0, 1, f32)
         across = swap(across, "tp", tp_size, 2)
         beside = swap(beside, "grp", grp_size, 1)
         corner = lax.ppermute(corner, ("grp", "tp"), corner_pairs)
         results.append((own, across, beside, corner))
-    return final_sum(sp_size, results)
+    return final_sum(results)
+
+
+GROUPS = ((0, 1, 3), (2,))
 
 
 def is_short(sizes):

time: 69 us -> 68.6 us (level)
  the two profiles are of different devices: /device:TPU:24 before, /device:TPU:0 now
where the time goes in v2:
time: 68.6 us; the launch traced here: 68.3 us
  starting transfers between devices  34.5 us (50%)
  waiting for transfers between devices  27.4 us (40%)
  Pallas kernels  6 us (9%)
    ppermute x1, waiting for transfers between devices, fast_shards(): p1 = lax.ppermute(packed, 'sp', [(0, 1)])  8.7 us
    ppermute x1, starting transfers between devices, fast_shards(): p3 = lax.ppermute(packed, 'sp', [(0, 2)])  6.6 us
    ppermute x8, starting transfers between devices, swap(): return lax.ppermute(array, axis, [(k, k ^ d) for k in range(size)])  5.91 us
    ppermute x1, starting transfers between devices, fast_shards(): p1 = lax.ppermute(packed, 'sp', [(0, 1)])  5.05 us
    ppermute x8, waiting for transfers between devices, swap(): return lax.ppermute(array, axis, [(k, k ^ d) for k in range(size)])  4.99 us
    ppermute x1, waiting for transfers between devices, fast_shards(): weight_two = lax.ppermute(own_weight, 'sp', [(0, 2), (last, 1)])  4.88 us
    ppermute x1, waiting for transfers between devices, fast_shards(): weight_end = lax.ppermute(weight_mid, 'sp', [(1, 0), (2, last)])  4.17 us
    ppermute x1, starting transfers between devices, fast_shards(): weight_far = lax.ppermute(own_weight, 'sp', [(0, last), (last, 0)])  3.99 us
  transfers between devices with their start and end apart: 22, of which 7 were waited for; matrix products, arithmetic and copies ran while one was open for 0% of the time, Pallas kernels for 4%

profile of v2, /device:TPU:0, one launch (start us, length us, event | category | flops | bytes accessed | tf_op | source)
XLA Modules:
  0.0 68.3 jit_solution(5526472836476795547)
XLA Ops:
  0.0 2.3 %prepare.1 = (f32[256,256]{1,0:T(8,128)S(1)}, bf16[256,256]{1,0:T(8,128)(2,1)S(1)}, bf16[400,256]{1,0:T(8,128)(2,1)S(1)}, bf16[512,256]{1,0:T(8,128)(2,1)S(1)}, ...) custom-call(bf16[64,256]{1,0:T(8,128)(2,1)} %bitcast.7, bf16[64,256]{1,0:T(8,128)(2,1)} %bitcast.8, ...), custom_call_target="tpu_custom_call" | custom-call | flops 134217728 | bytes 1385480 | tf_op jit(solution)/shard_map/prepare/pallas_call | solution.py:448
  3.0 6.6 %collective-permute-start.2 = (bf16[400,256]{1,0:T(8,128)(2,1)S(1)}, bf16[400,256]{1,0:T(8,128)(2,1)S(1)}, u32[]{:S(2)}, u32[]{:S(2)}) collective-permute-start(bf16[400,256]{1,0:T(8,128)(2,1)S(1)} %get-tuple-element.23.own_ref), channel_id=1, source_target_pairs={{0,8},{1,9},{2,10},{3,11},{16,24},{17,25},{18,26},{19,27}} | collective-permute-start | bytes 614408 | tf_op jit(solution)/shard_map/ppermute | solution.py:700
  9.6 0.7 collective-permute-start.5
  10.4 4.0 %collective-permute-start.10 = (bf16[2,256,256]{2,1,0:T(8,128)(2,1)S(1)}, bf16[2,256,256]{2,1,0:T(8,128)(2,1)S(1)}, u32[]{:S(2)}, u32[]{:S(2)}) collective-permute-start(bf16[2,256,256]{2,1,0:T(8,128)(2,1)S(1)} %constant_dynamic-slice_fusion.refs_6_), channel_id=1, source_target_pairs={{0,12},{12,0},{1,13},{13,1},{2,14},{14,2},{3,15},{15,3},{16,28},{2... | collective-permute-start | bytes 786440 | tf_op jit(solution)/shard_map/ppermute | solution.py:707
  14.4 5.0 %collective-permute-start = (bf16[400,256]{1,0:T(8,128)(2,1)S(1)}, bf16[400,256]{1,0:T(8,128)(2,1)S(1)}, u32[]{:S(2)}, u32[]{:S(2)}) collective-permute-start(bf16[400,256]{1,0:T(8,128)(2,1)S(1)} %get-tuple-element.23.own_ref), channel_id=1, source_target_pairs={{0,4},{1,5},{2,6},{3,7},{16,20},{17,21},{18,22},{19,23}} | collective-permute-start | bytes 614408 | tf_op jit(solution)/shard_map/ppermute | solution.py:698
  19.4 0.7 collective-permute-start.11
  20.9 8.7 %collective-permute-done.p1_ref = bf16[400,256]{1,0:T(8,128)(2,1)S(1)} collective-permute-done((bf16[400,256]{1,0:T(8,128)(2,1)S(1)}, bf16[400,256]{1,0:T(8,128)(2,1)S(1)}, u32[]{:S(2)}, u32[]{:S(2)}) %collective-permute-start) | collective-permute-done | bytes 204832 | tf_op jit(solution)/shard_map/ppermute | solution.py:698
  29.6 1.3 %shard_map.137.refs_2_ = bf16[256,256]{1,0:T(8,128)(2,1)S(1)} custom-call(bf16[256,256]{1,0:T(8,128)(2,1)S(1)} %get-tuple-element.27.asked_ref, bf16[400,256]{1,0:T(8,128)(2,1)S(1)} %get-tuple-element.23.own_ref, bf16[400,256]{1,0:T(8,128)(2,1)S(1)} %collective-permute-done.p1_ref, bf16[400,256]{1,0:T(8,128)(2,1)S(1)} %collective-permute-done.1.one_ref.p2_ref, ...), custom_call_target="tpu_custom_call" | custom-call | flops 402653184 | bytes 951304 | tf_op jit(solution)/shard_map/pallas_call | solution.py:583
  30.9 3.4 %collective-permute-start.6 = (bf16[256,256]{1,0:T(8,128)(2,1)S(1)}, bf16[256,256]{1,0:T(8,128)(2,1)S(1)}, u32[]{:S(2)}, u32[]{:S(2)}) collective-permute-start(bf16[256,256]{1,0:T(8,128)(2,1)S(1)} %shard_map.137.refs_2_), channel_id=1, source_target_pairs={{0,16},{4,20},{8,24},{16,0},{20,4},{24,8},{1,17},{5,21},{9,25},{17... | collective-permute-start | bytes 393224 | tf_op jit(solution)/shard_map/ppermute | solution.py:726
  36.6 1.5 %collective-permute-done.6.refs_3_ = bf16[256,256]{1,0:T(8,128)(2,1)S(1)} collective-permute-done((bf16[256,256]{1,0:T(8,128)(2,1)S(1)}, bf16[256,256]{1,0:T(8,128)(2,1)S(1)}, u32[]{:S(2)}, u32[]{:S(2)}) %collective-permute-start.6) | collective-permute-done | bytes 131104 | tf_op jit(solution)/shard_map/ppermute | solution.py:726
  38.1 3.0 %collective-permute-done.4.refs_1_ = bf16[256,256]{1,0:T(8,128)(2,1)S(1)} collective-permute-done((bf16[256,256]{1,0:T(8,128)(2,1)S(1)}, bf16[256,256]{1,0:T(8,128)(2,1)S(1)}, u32[]{:S(2)}, u32[]{:S(2)}) %collective-permute-start.4) | collective-permute-done | bytes 131104 | tf_op jit(solution)/shard_map/ppermute | solution.py:693
  41.5 1.7 %collective-permute-start.17 = (bf16[2,256,256]{2,1,0:T(8,128)(2,1)S(1)}, bf16[2,256,256]{2,1,0:T(8,128)(2,1)S(1)}, u32[]{:S(2)}, u32[]{:S(2)}) collective-permute-start(bf16[2,256,256]{2,1,0:T(8,128)(2,1)S(1)} %constant_dynamic-slice_fusion.refs_6_), channel_id=1, source_target_pairs={{0,8},{12,4},{1,9},{13,5},{2,10},{14,6},{3,11},{15,7},{16,24},{28,... | collective-permute-start | bytes 786440 | tf_op jit(solution)/shard_map/ppermute | solution.py:708
  43.2 1.3 %collective-permute-start.16 = (bf16[2,256,256]{2,1,0:T(8,128)(2,1)S(1)}, bf16[2,256,256]{2,1,0:T(8,128)(2,1)S(1)}, u32[]{:S(2)}, u32[]{:S(2)}) collective-permute-start(bf16[2,256,256]{2,1,0:T(8,128)(2,1)S(1)} %collective-permute-done.11.refs_9_), channel_id=1, source_target_pairs={{4,0},{8,12},{5,1},{9,13},{6,2},{10,14},{7,3},{11,15},{20,16},{24,... | collective-permute-start | bytes 786440 | tf_op jit(solution)/shard_map/ppermute | solution.py:709
  44.5 4.9 %collective-permute-done.17.refs_7_ = bf16[2,256,256]{2,1,0:T(8,128)(2,1)S(1)} collective-permute-done((bf16[2,256,256]{2,1,0:T(8,128)(2,1)S(1)}, bf16[2,256,256]{2,1,0:T(8,128)(2,1)S(1)}, u32[]{:S(2)}, u32[]{:S(2)}) %collective-permute-start.17) | collective-permute-done | bytes 262176 | tf_op jit(solution)/shard_map/ppermute | solution.py:708
  49.4 4.2 %collective-permute-done.16.refs_6_ = bf16[2,256,256]{2,1,0:T(8,128)(2,1)S(1)} collective-permute-done((bf16[2,256,256]{2,1,0:T(8,128)(2,1)S(1)}, bf16[2,256,256]{2,1,0:T(8,128)(2,1)S(1)}, u32[]{:S(2)}, u32[]{:S(2)}) %collective-permute-start.16) | collective-permute-done | bytes 262176 | tf_op jit(solution)/shard_map/ppermute | solution.py:709
  54.3 1.6 %collective-permute-start.13 = (bf16[64,768]{1,0:T(8,128)(2,1)S(1)}, bf16[64,768]{1,0:T(8,128)(2,1)S(1)}, u32[]{:S(2)}, u32[]{:S(2)}) collective-permute-start(bf16[64,768]{1,0:T(8,128)(2,1)S(1)} %get-tuple-element.29), channel_id=1, source_target_pairs={{0,2},{1,3},{2,0},{3,1},{4,6},{5,7},{6,4},{7,5},{8,10},{9,11},{10,... | collective-permute-start | bytes 294920 | tf_op jit(solution)/shard_map/ppermute | solution.py:693
  55.8 1.0 %collective-permute-start.14 = (bf16[64,768]{1,0:T(8,128)(2,1)S(1)}, bf16[64,768]{1,0:T(8,128)(2,1)S(1)}, u32[]{:S(2)}, u32[]{:S(2)}) collective-permute-start(bf16[64,768]{1,0:T(8,128)(2,1)S(1)} %get-tuple-element.30), channel_id=1, source_target_pairs={{0,16},{16,0},{1,17},{17,1},{2,18},{18,2},{3,19},{19,3},{4,20},{20... | collective-permute-start | bytes 294920 | tf_op jit(solution)/shard_map/ppermute | solution.py:693
  56.9 1.0 %collective-permute-start.15 = (bf16[64,768]{1,0:T(8,128)(2,1)S(1)}, bf16[64,768]{1,0:T(8,128)(2,1)S(1)}, u32[]{:S(2)}, u32[]{:S(2)}) collective-permute-start(bf16[64,768]{1,0:T(8,128)(2,1)S(1)} %get-tuple-element.31), channel_id=1, source_target_pairs={{0,18},{1,19},{2,16},{3,17},{16,2},{17,3},{18,0},{19,1},{4,22},{5,... | collective-permute-start | bytes 294920 | tf_op jit(solution)/shard_map/ppermute | solution.py:751
  58.1 1.6 %collective-permute-start.19 = (bf16[64,256]{1,0:T(8,128)(2,1)S(1)}, bf16[64,256]{1,0:T(8,128)(2,1)S(1)}, u32[]{:S(2)}, u32[]{:S(2)}) collective-permute-start(bf16[64,256]{1,0:T(8,128)(2,1)S(1)} %get-tuple-element.32), channel_id=1, source_target_pairs={{0,2},{1,3},{2,0},{3,1},{4,6},{5,7},{6,4},{7,5},{8,10},{9,11},{10,... | collective-permute-start | bytes 98312 | tf_op jit(solution)/shard_map/ppermute | solution.py:693
  59.7 1.0 %collective-permute-start.20 = (bf16[64,256]{1,0:T(8,128)(2,1)S(1)}, bf16[64,256]{1,0:T(8,128)(2,1)S(1)}, u32[]{:S(2)}, u32[]{:S(2)}) collective-permute-start(bf16[64,256]{1,0:T(8,128)(2,1)S(1)} %get-tuple-element.33), channel_id=1, source_target_pairs={{0,16},{16,0},{1,17},{17,1},{2,18},{18,2},{3,19},{19,3},{4,20},{20... | collective-permute-start | bytes 98312 | tf_op jit(solution)/shard_map/ppermute | solution.py:693
  60.7 2.0 %collective-permute-done.19.refs_5_ = bf16[64,256]{1,0:T(8,128)(2,1)S(1)} collective-permute-done((bf16[64,256]{1,0:T(8,128)(2,1)S(1)}, bf16[64,256]{1,0:T(8,128)(2,1)S(1)}, u32[]{:S(2)}, u32[]{:S(2)}) %collective-permute-start.19) | collective-permute-done | bytes 32800 | tf_op jit(solution)/shard_map/ppermute | solution.py:693
  62.7 1.6 %collective-permute-start.21 = (bf16[64,256]{1,0:T(8,128)(2,1)S(1)}, bf16[64,256]{1,0:T(8,128)(2,1)S(1)}, u32[]{:S(2)}, u32[]{:S(2)}) collective-permute-start(bf16[64,256]{1,0:T(8,128)(2,1)S(1)} %get-tuple-element.34), channel_id=1, source_target_pairs={{0,18},{1,19},{2,16},{3,17},{16,2},{17,3},{18,0},{19,1},{4,22},{5,... | collective-permute-start | bytes 98312 | tf_op jit(solution)/shard_map/ppermute | solution.py:751
  64.3 3.2 %collective-permute-done.21.refs_7_ = bf16[64,256]{1,0:T(8,128)(2,1)S(1)} collective-permute-done((bf16[64,256]{1,0:T(8,128)(2,1)S(1)}, bf16[64,256]{1,0:T(8,128)(2,1)S(1)}, u32[]{:S(2)}, u32[]{:S(2)}) %collective-permute-start.21) | collective-permute-done | bytes 32800 | tf_op jit(solution)/shard_map/ppermute | solution.py:751
  67.5 0.8 %final.1 = bf16[64,2048]{1,0:T(8,128)(2,1)} custom-call(f32[64,768]{1,0:T(8,128)S(1)} %pair.4.refs_0_, bf16[64,768]{1,0:T(8,128)(2,1)S(1)} %collective-permute-done.13.refs_1_, bf16[64,768]{1,0:T(8,128)(2,1)S(1)} %collective-permute-done.14.refs_2_, bf16[64,768]{1,0:T(8,128)(2,1)S(1)} %collective-permute-done.15.refs_3_, f32[64,256]{1,0:T(8,128)S(1)} %pair.6.refs_4_, ...), custom_call_target="tpu_custom_call" | custom-call | flops 131072 | bytes 917504 | tf_op jit(solution)/shard_map/final/pallas_call | solution.py:678
  (37 shorter events, 5.2 us)
Async XLA Ops:
  0.0 10.2 %copy-start = (bf16[2,256,512]{2,1,0:T(8,128)(2,1)S(1)}, bf16[2,256,512]{2,1,0:T(8,128)(2,1)}, u32[]{:S(2)}) copy-start(bf16[2,256,512]{2,1,0:T(8,128)(2,1)} %param.27) | copy-start | bytes 1572868
  2.3 12.1 %collective-permute-start.1 = (bf16[400,256]{1,0:T(8,128)(2,1)S(1)}, bf16[400,256]{1,0:T(8,128)(2,1)S(1)}, u32[]{:S(2)}, u32[]{:S(2)}) collective-permute-start(bf16[400,256]{1,0:T(8,128)(2,1)S(1)} %get-tuple-element.23.own_ref), channel_id=1, source_target_pairs={{4,8},{5,9},{6,10},{7,11},{20,24},{21,25},{22,26},{23,27}} | collective-permute-start | bytes 614408 | tf_op jit(solution)/shard_map/ppermute | solution.py:699
  3.0 16.5 %collective-permute-start.2 = (bf16[400,256]{1,0:T(8,128)(2,1)S(1)}, bf16[400,256]{1,0:T(8,128)(2,1)S(1)}, u32[]{:S(2)}, u32[]{:S(2)}) collective-permute-start(bf16[400,256]{1,0:T(8,128)(2,1)S(1)} %get-tuple-element.23.own_ref), channel_id=1, source_target_pairs={{0,8},{1,9},{2,10},{3,11},{16,24},{17,25},{18,26},{19,27}} | collective-permute-start | bytes 614408 | tf_op jit(solution)/shard_map/ppermute | solution.py:700
  9.6 10.6 %collective-permute-start.5 = (bf16[512,256]{1,0:T(8,128)(2,1)S(1)}, bf16[512,256]{1,0:T(8,128)(2,1)S(1)}, u32[]{:S(2)}, u32[]{:S(2)}) collective-permute-start(bf16[512,256]{1,0:T(8,128)(2,1)S(1)} %get-tuple-element.24), channel_id=1, source_target_pairs={{12,8},{13,9},{14,10},{15,11},{28,24},{29,25},{30,26},{31,27}} | collective-permute-start | bytes 786440 | tf_op jit(solution)/shard_map/ppermute | solution.py:697
  10.3 25.0 %collective-permute-start.9 = (bf16[2,256,256]{2,1,0:T(8,128)(2,1)S(1)}, bf16[2,256,256]{2,1,0:T(8,128)(2,1)S(1)}, u32[]{:S(2)}, u32[]{:S(2)}) collective-permute-start(bf16[2,256,256]{2,1,0:T(8,128)(2,1)S(1)} %constant_dynamic-slice_fusion.refs_6_), channel_id=1, source_target_pairs={{0,4},{4,0},{8,12},{12,8},{1,5},{5,1},{9,13},{13,9},{2,6},{6,2},{1... | collective-permute-start | bytes 786440 | tf_op jit(solution)/shard_map/ppermute | solution.py:693
  10.4 25.6 %collective-permute-start.10 = (bf16[2,256,256]{2,1,0:T(8,128)(2,1)S(1)}, bf16[2,256,256]{2,1,0:T(8,128)(2,1)S(1)}, u32[]{:S(2)}, u32[]{:S(2)}) collective-permute-start(bf16[2,256,256]{2,1,0:T(8,128)(2,1)S(1)} %constant_dynamic-slice_fusion.refs_6_), channel_id=1, source_target_pairs={{0,12},{12,0},{1,13},{13,1},{2,14},{14,2},{3,15},{15,3},{16,28},{2... | collective-permute-start | bytes 786440 | tf_op jit(solution)/shard_map/ppermute | solution.py:707
  14.4 15.2 %collective-permute-start = (bf16[400,256]{1,0:T(8,128)(2,1)S(1)}, bf16[400,256]{1,0:T(8,128)(2,1)S(1)}, u32[]{:S(2)}, u32[]{:S(2)}) collective-permute-start(bf16[400,256]{1,0:T(8,128)(2,1)S(1)} %get-tuple-element.23.own_ref), channel_id=1, source_target_pairs={{0,4},{1,5},{2,6},{3,7},{16,20},{17,21},{18,22},{19,23}} | collective-permute-start | bytes 614408 | tf_op jit(solution)/shard_map/ppermute | solution.py:698
  19.4 17.2 %collective-permute-start.11 = (bf16[2,256,256]{2,1,0:T(8,128)(2,1)S(1)}, bf16[2,256,256]{2,1,0:T(8,128)(2,1)S(1)}, u32[]{:S(2)}, u32[]{:S(2)}) collective-permute-start(bf16[2,256,256]{2,1,0:T(8,128)(2,1)S(1)} %constant_dynamic-slice_fusion.refs_6_), channel_id=1, source_target_pairs={{4,8},{8,4},{5,9},{9,5},{6,10},{10,6},{7,11},{11,7},{20,24},{24,20... | collective-permute-start | bytes 786440 | tf_op jit(solution)/shard_map/ppermute | solution.py:706
  20.2 14.1 %collective-permute-start.3 = (bf16[128,256]{1,0:T(8,128)(2,1)S(1)}, bf16[128,256]{1,0:T(8,128)(2,1)S(1)}, u32[]{:S(2)}, u32[]{:S(2)}) collective-permute-start(bf16[128,256]{1,0:T(8,128)(2,1)S(1)} %blend.1), channel_id=1, source_target_pairs={{8,12},{9,13},{10,14},{11,15},{24,28},{25,29},{26,30},{27,31}} | collective-permute-start | bytes 196616 | tf_op jit(solution)/shard_map/ppermute | solution.py:710
  30.9 7.2 %collective-permute-start.6 = (bf16[256,256]{1,0:T(8,128)(2,1)S(1)}, bf16[256,256]{1,0:T(8,128)(2,1)S(1)}, u32[]{:S(2)}, u32[]{:S(2)}) collective-permute-start(bf16[256,256]{1,0:T(8,128)(2,1)S(1)} %shard_map.137.refs_2_), channel_id=1, source_target_pairs={{0,16},{4,20},{8,24},{16,0},{20,4},{24,8},{1,17},{5,21},{9,25},{17... | collective-permute-start | bytes 393224 | tf_op jit(solution)/shard_map/ppermute | solution.py:726
  34.3 3.8 %collective-permute-start.7 = (bf16[256,256]{1,0:T(8,128)(2,1)S(1)}, bf16[256,256]{1,0:T(8,128)(2,1)S(1)}, u32[]{:S(2)}, u32[]{:S(2)}) collective-permute-start(bf16[256,256]{1,0:T(8,128)(2,1)S(1)} %shard_map.136), channel_id=1, source_target_pairs={{8,12},{9,13},{10,14},{11,15},{24,28},{25,29},{26,30},{27,31}} | collective-permute-start | bytes 393224 | tf_op jit(solution)/shard_map/ppermute | solution.py:713
  35.3 2.7 %collective-permute-start.8 = (bf16[256,256]{1,0:T(8,128)(2,1)S(1)}, bf16[256,256]{1,0:T(8,128)(2,1)S(1)}, u32[]{:S(2)}, u32[]{:S(2)}) collective-permute-start(bf16[256,256]{1,0:T(8,128)(2,1)S(1)} %shard_map.136), channel_id=1, source_target_pairs={{8,28},{24,12},{9,29},{25,13},{10,30},{26,14},{11,31},{27,15}} | collective-permute-start | bytes 393224 | tf_op jit(solution)/shard_map/ppermute | solution.py:728
  36.0 5.0 %collective-permute-start.4 = (bf16[256,256]{1,0:T(8,128)(2,1)S(1)}, bf16[256,256]{1,0:T(8,128)(2,1)S(1)}, u32[]{:S(2)}, u32[]{:S(2)}) collective-permute-start(bf16[256,256]{1,0:T(8,128)(2,1)S(1)} %carry.1.refs_0_), channel_id=1, source_target_pairs={{0,16},{16,0},{1,17},{17,1},{2,18},{18,2},{3,19},{19,3},{4,20},{20... | collective-permute-start | bytes 393224 | tf_op jit(solution)/shard_map/ppermute | solution.py:693
  41.4 12.8 %collective-permute-start.12 = (bf16[256,768]{1,0:T(8,128)(2,1)S(1)}, bf16[256,768]{1,0:T(8,128)(2,1)S(1)}, u32[]{:S(2)}, u32[]{:S(2)}) collective-permute-start(bf16[256,768]{1,0:T(8,128)(2,1)S(1)} %project.5), channel_id=1, source_target_pairs={{0,1},{1,0},{2,3},{3,2},{4,5},{5,4},{6,7},{7,6},{8,9},{9,8},{10,11... | collective-permute-start | bytes 1179656 | tf_op jit(solution)/shard_map/ppermute | solution.py:693
  41.5 7.8 %collective-permute-start.17 = (bf16[2,256,256]{2,1,0:T(8,128)(2,1)S(1)}, bf16[2,256,256]{2,1,0:T(8,128)(2,1)S(1)}, u32[]{:S(2)}, u32[]{:S(2)}) collective-permute-start(bf16[2,256,256]{2,1,0:T(8,128)(2,1)S(1)} %constant_dynamic-slice_fusion.refs_6_), channel_id=1, source_target_pairs={{0,8},{12,4},{1,9},{13,5},{2,10},{14,6},{3,11},{15,7},{16,24},{28,... | collective-permute-start | bytes 786440 | tf_op jit(solution)/shard_map/ppermute | solution.py:708
  43.2 10.4 %collective-permute-start.16 = (bf16[2,256,256]{2,1,0:T(8,128)(2,1)S(1)}, bf16[2,256,256]{2,1,0:T(8,128)(2,1)S(1)}, u32[]{:S(2)}, u32[]{:S(2)}) collective-permute-start(bf16[2,256,256]{2,1,0:T(8,128)(2,1)S(1)} %collective-permute-done.11.refs_9_), channel_id=1, source_target_pairs={{4,0},{8,12},{5,1},{9,13},{6,2},{10,14},{7,3},{11,15},{20,16},{24,... | collective-permute-start | bytes 786440 | tf_op jit(solution)/shard_map/ppermute | solution.py:709
  53.8 4.3 %collective-permute-start.18 = (bf16[256,256]{1,0:T(8,128)(2,1)S(1)}, bf16[256,256]{1,0:T(8,128)(2,1)S(1)}, u32[]{:S(2)}, u32[]{:S(2)}) collective-permute-start(bf16[256,256]{1,0:T(8,128)(2,1)S(1)} %project.7), channel_id=1, source_target_pairs={{0,1},{1,0},{2,3},{3,2},{4,5},{5,4},{6,7},{7,6},{8,9},{9,8},{10,11... | collective-permute-start | bytes 393224 | tf_op jit(solution)/shard_map/ppermute | solution.py:693
  54.3 13.2 %collective-permute-start.13 = (bf16[64,768]{1,0:T(8,128)(2,1)S(1)}, bf16[64,768]{1,0:T(8,128)(2,1)S(1)}, u32[]{:S(2)}, u32[]{:S(2)}) collective-permute-start(bf16[64,768]{1,0:T(8,128)(2,1)S(1)} %get-tuple-element.29), channel_id=1, source_target_pairs={{0,2},{1,3},{2,0},{3,1},{4,6},{5,7},{6,4},{7,5},{8,10},{9,11},{10,... | collective-permute-start | bytes 294920 | tf_op jit(solution)/shard_map/ppermute | solution.py:693
  55.8 11.7 %collective-permute-start.14 = (bf16[64,768]{1,0:T(8,128)(2,1)S(1)}, bf16[64,768]{1,0:T(8,128)(2,1)S(1)}, u32[]{:S(2)}, u32[]{:S(2)}) collective-permute-start(bf16[64,768]{1,0:T(8,128)(2,1)S(1)} %get-tuple-element.30), channel_id=1, source_target_pairs={{0,16},{16,0},{1,17},{17,1},{2,18},{18,2},{3,19},{19,3},{4,20},{20... | collective-permute-start | bytes 294920 | tf_op jit(solution)/shard_map/ppermute | solution.py:693
  56.9 10.7 %collective-permute-start.15 = (bf16[64,768]{1,0:T(8,128)(2,1)S(1)}, bf16[64,768]{1,0:T(8,128)(2,1)S(1)}, u32[]{:S(2)}, u32[]{:S(2)}) collective-permute-start(bf16[64,768]{1,0:T(8,128)(2,1)S(1)} %get-tuple-element.31), channel_id=1, source_target_pairs={{0,18},{1,19},{2,16},{3,17},{16,2},{17,3},{18,0},{19,1},{4,22},{5,... | collective-permute-start | bytes 294920 | tf_op jit(solution)/shard_map/ppermute | solution.py:751
  58.1 4.6 %collective-permute-start.19 = (bf16[64,256]{1,0:T(8,128)(2,1)S(1)}, bf16[64,256]{1,0:T(8,128)(2,1)S(1)}, u32[]{:S(2)}, u32[]{:S(2)}) collective-permute-start(bf16[64,256]{1,0:T(8,128)(2,1)S(1)} %get-tuple-element.32), channel_id=1, source_target_pairs={{0,2},{1,3},{2,0},{3,1},{4,6},{5,7},{6,4},{7,5},{8,10},{9,11},{10,... | collective-permute-start | bytes 98312 | tf_op jit(solution)/shard_map/ppermute | solution.py:693
  59.7 4.7 %collective-permute-start.20 = (bf16[64,256]{1,0:T(8,128)(2,1)S(1)}, bf16[64,256]{1,0:T(8,128)(2,1)S(1)}, u32[]{:S(2)}, u32[]{:S(2)}) collective-permute-start(bf16[64,256]{1,0:T(8,128)(2,1)S(1)} %get-tuple-element.33), channel_id=1, source_target_pairs={{0,16},{16,0},{1,17},{17,1},{2,18},{18,2},{3,19},{19,3},{4,20},{20... | collective-permute-start | bytes 98312 | tf_op jit(solution)/shard_map/ppermute | solution.py:693
  62.7 4.8 %collective-permute-start.21 = (bf16[64,256]{1,0:T(8,128)(2,1)S(1)}, bf16[64,256]{1,0:T(8,128)(2,1)S(1)}, u32[]{:S(2)}, u32[]{:S(2)}) collective-permute-start(bf16[64,256]{1,0:T(8,128)(2,1)S(1)} %get-tuple-element.34), channel_id=1, source_target_pairs={{0,18},{1,19},{2,16},{3,17},{16,2},{17,3},{18,0},{19,1},{4,22},{5,... | collective-permute-start | bytes 98312 | tf_op jit(solution)/shard_map/ppermute | solution.py:751

commit v3 on v2

--- a/solution.py
+++ b/solution.py
@@ -705,25 +705,23 @@
     weight_one = swap(own_weight, "sp", sp_size, 1)
     weight_mid = lax.ppermute(own_weight, "sp", [(1, 2), (2, 1)])
     weight_far = lax.ppermute(own_weight, "sp", [(0, last), (last, 0)])
-    weight_two = lax.ppermute(own_weight, "sp", [(0, 2), (last, 1)])
+    weight_two = lax.ppermute(weight_one, "sp", [(1, 2), (2, 1)])
     weight_end = lax.ppermute(weight_mid, "sp", [(1, 0), (2, last)])
     p4 = lax.ppermute(blend(packed, p2, p3), "sp", [(2, last)])
     helped = attention(helper_kernel, last, tokens, packed, p0, p2, p3, weight, gains)
     helped, asked = lax.optimization_barrier((helped, asked))
     p5 = lax.ppermute(helped, "sp", [(2, last)])
+    recurrent = carry_in(local, faded, gains, p1, p2, p3, p4)
+    recurrent, asked = lax.optimization_barrier((recurrent, asked))
     main = attention(main_kernel, last, tokens, asked, packed, p1, p2, p3, weight, gains)
-    recurrent = carry_in(local, faded, gains, p1, p2, p3, p4)
     ends = [
         (g * sp_size + last - 1, (g ^ 1) * sp_size + last) for g in range(grp_size)
-    ]
-    others = [
-        (g * sp_size + k, (g ^ 1) * sp_size + k) for g in range(grp_size) for k in range(last)
     ]
     mixed = (
         recurrent,
         swap(recurrent, "grp", grp_size, 1),
         main,
-        lax.ppermute(main, ("grp", "sp"), others),
+        swap(main, "grp", grp_size, 1),
         p5,
         lax.ppermute(helped, ("grp", "sp"), ends),
     )

time: 68.6 us -> 67.4 us (0.983)
  the two profiles are of different devices: /device:TPU:0 before, /device:TPU:16 now
where the time goes in v3:
time: 67.4 us; the launch traced here: 67.1 us
  starting transfers between devices  32.8 us (49%)
  waiting for transfers between devices  25.6 us (38%)
  Pallas kernels  8.45 us (13%)
    ppermute x9, starting transfers between devices, swap(): return lax.ppermute(array, axis, [(k, k ^ d) for k in range(size)])  11.1 us
    ppermute x9, waiting for transfers between devices, swap(): return lax.ppermute(array, axis, [(k, k ^ d) for k in range(size)])  6.87 us
    ppermute x1, waiting for transfers between devices, fast_shards(): p2 = lax.ppermute(packed, 'sp', [(1, 2)])  5.76 us
    ppermute x1, starting transfers between devices, fast_shards(): lax.ppermute(helped, ('grp', 'sp'), ends)  5.48 us
    ppermute x1, waiting for transfers between devices, fast_shards(): weight_end = lax.ppermute(weight_mid, 'sp', [(1, 0), (2, last)])  4.25 us
    ppermute x1, waiting for transfers between devices, fast_shards(): weight_two = lax.ppermute(weight_one, 'sp', [(1, 2), (2, 1)])  4.13 us
    pallas_call x2, Pallas kernels, attention(): pl.pallas_call(functools.partial(kernel, last), out_shape=jax.ShapeDtypeS...  3.76 us
    ppermute x2, starting transfers between devices, fast_shards(): corner = lax.ppermute(corner, ('grp', 'tp'), corner_pairs)  2.64 us
  transfers between devices with their start and end apart: 22, of which 8 were waited for; matrix products, arithmetic and copies ran while one was open for 0% of the time, Pallas kernels for 8%

profile of v3, /device:TPU:16, one launch (start us, length us, event | category | flops | bytes accessed | tf_op | source)
XLA Modules:
  0.0 67.1 jit_solution(10015757481179260163)
XLA Ops:
  0.0 2.3 %prepare.1 = (f32[256,256]{1,0:T(8,128)S(1)}, bf16[256,256]{1,0:T(8,128)(2,1)S(1)}, bf16[400,256]{1,0:T(8,128)(2,1)S(1)}, bf16[512,256]{1,0:T(8,128)(2,1)S(1)}, ...) custom-call(bf16[64,256]{1,0:T(8,128)(2,1)} %bitcast.7, bf16[64,256]{1,0:T(8,128)(2,1)} %bitcast.8, ...), custom_call_target="tpu_custom_call" | custom-call | flops 134217728 | bytes 1385480 | tf_op jit(solution)/shard_map/prepare/pallas_call | solution.py:448
  6.2 2.7 %collective-permute-start.9 = (bf16[2,256,256]{2,1,0:T(8,128)(2,1)S(1)}, bf16[2,256,256]{2,1,0:T(8,128)(2,1)S(1)}, u32[]{:S(2)}, u32[]{:S(2)}) collective-permute-start(bf16[2,256,256]{2,1,0:T(8,128)(2,1)S(1)} %constant_dynamic-slice_fusion.refs_6_), channel_id=1, source_target_pairs={{0,4},{4,0},{8,12},{12,8},{1,5},{5,1},{9,13},{13,9},{2,6},{6,2},{1... | collective-permute-start | bytes 786440 | tf_op jit(solution)/shard_map/ppermute | solution.py:693
  9.6 5.8 %collective-permute-done.1.one_ref.p2_ref = bf16[400,256]{1,0:T(8,128)(2,1)S(1)} collective-permute-done((bf16[400,256]{1,0:T(8,128)(2,1)S(1)}, bf16[400,256]{1,0:T(8,128)(2,1)S(1)}, u32[]{:S(2)}, u32[]{:S(2)}) %collective-permute-start.1) | collective-permute-done | bytes 204832 | tf_op jit(solution)/shard_map/ppermute | solution.py:699
  16.1 2.1 %collective-permute-start.11 = (bf16[2,256,256]{2,1,0:T(8,128)(2,1)S(1)}, bf16[2,256,256]{2,1,0:T(8,128)(2,1)S(1)}, u32[]{:S(2)}, u32[]{:S(2)}) collective-permute-start(bf16[2,256,256]{2,1,0:T(8,128)(2,1)S(1)} %constant_dynamic-slice_fusion.refs_6_), channel_id=1, source_target_pairs={{4,8},{8,4},{5,9},{9,5},{6,10},{10,6},{7,11},{11,7},{20,24},{24,20... | collective-permute-start | bytes 786440 | tf_op jit(solution)/shard_map/ppermute | solution.py:706
  18.2 1.3 %collective-permute-start.3 = (bf16[128,256]{1,0:T(8,128)(2,1)S(1)}, bf16[128,256]{1,0:T(8,128)(2,1)S(1)}, u32[]{:S(2)}, u32[]{:S(2)}) collective-permute-start(bf16[128,256]{1,0:T(8,128)(2,1)S(1)} %blend.1), channel_id=1, source_target_pairs={{8,12},{9,13},{10,14},{11,15},{24,28},{25,29},{26,30},{27,31}} | collective-permute-start | bytes 196616 | tf_op jit(solution)/shard_map/ppermute | solution.py:710
  19.5 2.1 %shard_map.136 = bf16[256,256]{1,0:T(8,128)(2,1)S(1)} custom-call(bf16[400,256]{1,0:T(8,128)(2,1)S(1)} %get-tuple-element.25.own_ref, bf16[512,256]{1,0:T(8,128)(2,1)S(1)} %collective-permute-done.4.p1_ref, bf16[400,256]{1,0:T(8,128)(2,1)S(1)} %collective-permute-done.1.one_ref.p2_ref, bf16[400,256]{1,0:T(8,128)(2,1)S(1)} %collective-permute-done.2.two_ref.p3_ref, ...), custom_call_target="tpu_custom_call" | custom-call | flops 402653184 | bytes 877576 | tf_op jit(solution)/shard_map/pallas_call | solution.py:583
  21.6 1.3 %collective-permute-start.7 = (bf16[256,256]{1,0:T(8,128)(2,1)S(1)}, bf16[256,256]{1,0:T(8,128)(2,1)S(1)}, u32[]{:S(2)}, u32[]{:S(2)}) collective-permute-start(bf16[256,256]{1,0:T(8,128)(2,1)S(1)} %shard_map.136), channel_id=1, source_target_pairs={{8,12},{9,13},{10,14},{11,15},{24,28},{25,29},{26,30},{27,31}} | collective-permute-start | bytes 393224 | tf_op jit(solution)/shard_map/ppermute | solution.py:713
  22.9 1.9 %collective-permute-done.3.p4_ref = bf16[128,256]{1,0:T(8,128)(2,1)S(1)} collective-permute-done((bf16[128,256]{1,0:T(8,128)(2,1)S(1)}, bf16[128,256]{1,0:T(8,128)(2,1)S(1)}, u32[]{:S(2)}, u32[]{:S(2)}) %collective-permute-start.3) | collective-permute-done | bytes 65568 | tf_op jit(solution)/shard_map/ppermute | solution.py:710
  24.8 5.5 %collective-permute-start.8 = (bf16[256,256]{1,0:T(8,128)(2,1)S(1)}, bf16[256,256]{1,0:T(8,128)(2,1)S(1)}, u32[]{:S(2)}, u32[]{:S(2)}) collective-permute-start(bf16[256,256]{1,0:T(8,128)(2,1)S(1)} %shard_map.136), channel_id=1, source_target_pairs={{8,28},{24,12},{9,29},{25,13},{10,30},{26,14},{11,31},{27,15}} | collective-permute-start | bytes 393224 | tf_op jit(solution)/shard_map/ppermute | solution.py:726
  30.6 1.7 %shard_map.137.refs_2_ = bf16[256,256]{1,0:T(8,128)(2,1)S(1)} custom-call(bf16[256,256]{1,0:T(8,128)(2,1)S(1)} %get-tuple-element.31.asked_ref, bf16[400,256]{1,0:T(8,128)(2,1)S(1)} %get-tuple-element.25.own_ref, bf16[400,256]{1,0:T(8,128)(2,1)S(1)} %collective-permute-done.p1_ref, bf16[400,256]{1,0:T(8,128)(2,1)S(1)} %collective-permute-done.1.one_ref.p2_ref, ...), custom_call_target="tpu_custom_call" | custom-call | flops 402653184 | bytes 951304 | tf_op jit(solution)/shard_map/pallas_call | solution.py:583
  32.9 1.5 %collective-permute-start.6 = (bf16[256,256]{1,0:T(8,128)(2,1)S(1)}, bf16[256,256]{1,0:T(8,128)(2,1)S(1)}, u32[]{:S(2)}, u32[]{:S(2)}) collective-permute-start(bf16[256,256]{1,0:T(8,128)(2,1)S(1)} %shard_map.137.refs_2_), channel_id=1, source_target_pairs={{0,16},{16,0},{1,17},{17,1},{2,18},{18,2},{3,19},{19,3},{4,20},{20... | collective-permute-start | bytes 393224 | tf_op jit(solution)/shard_map/ppermute | solution.py:693
  34.5 4.0 %collective-permute-done.5.refs_1_ = bf16[256,256]{1,0:T(8,128)(2,1)S(1)} collective-permute-done((bf16[256,256]{1,0:T(8,128)(2,1)S(1)}, bf16[256,256]{1,0:T(8,128)(2,1)S(1)}, u32[]{:S(2)}, u32[]{:S(2)}) %collective-permute-start.5) | collective-permute-done | bytes 131104 | tf_op jit(solution)/shard_map/ppermute | solution.py:693
  38.4 1.4 %collective-permute-done.6.refs_3_ = bf16[256,256]{1,0:T(8,128)(2,1)S(1)} collective-permute-done((bf16[256,256]{1,0:T(8,128)(2,1)S(1)}, bf16[256,256]{1,0:T(8,128)(2,1)S(1)}, u32[]{:S(2)}, u32[]{:S(2)}) %collective-permute-start.6) | collective-permute-done | bytes 131104 | tf_op jit(solution)/shard_map/ppermute | solution.py:693
  40.3 1.7 %collective-permute-start.16 = (bf16[2,256,256]{2,1,0:T(8,128)(2,1)S(1)}, bf16[2,256,256]{2,1,0:T(8,128)(2,1)S(1)}, u32[]{:S(2)}, u32[]{:S(2)}) collective-permute-start(bf16[2,256,256]{2,1,0:T(8,128)(2,1)S(1)} %collective-permute-done.11.refs_9_), channel_id=1, source_target_pairs={{4,0},{8,12},{5,1},{9,13},{6,2},{10,14},{7,3},{11,15},{20,16},{24,... | collective-permute-start | bytes 786440 | tf_op jit(solution)/shard_map/ppermute | solution.py:709
  42.0 1.9 %collective-permute-start.17 = (bf16[2,256,256]{2,1,0:T(8,128)(2,1)S(1)}, bf16[2,256,256]{2,1,0:T(8,128)(2,1)S(1)}, u32[]{:S(2)}, u32[]{:S(2)}) collective-permute-start(bf16[2,256,256]{2,1,0:T(8,128)(2,1)S(1)} %collective-permute-done.9.refs_7_), channel_id=1, source_target_pairs={{4,8},{8,4},{5,9},{9,5},{6,10},{10,6},{7,11},{11,7},{20,24},{24,20... | collective-permute-start | bytes 786440 | tf_op jit(solution)/shard_map/ppermute | solution.py:708
  44.0 4.3 %collective-permute-done.16.refs_6_ = bf16[2,256,256]{2,1,0:T(8,128)(2,1)S(1)} collective-permute-done((bf16[2,256,256]{2,1,0:T(8,128)(2,1)S(1)}, bf16[2,256,256]{2,1,0:T(8,128)(2,1)S(1)}, u32[]{:S(2)}, u32[]{:S(2)}) %collective-permute-start.16) | collective-permute-done | bytes 262176 | tf_op jit(solution)/shard_map/ppermute | solution.py:709
  48.2 4.1 %collective-permute-done.17.refs_7_ = bf16[2,256,256]{2,1,0:T(8,128)(2,1)S(1)} collective-permute-done((bf16[2,256,256]{2,1,0:T(8,128)(2,1)S(1)}, bf16[2,256,256]{2,1,0:T(8,128)(2,1)S(1)}, u32[]{:S(2)}, u32[]{:S(2)}) %collective-permute-start.17) | collective-permute-done | bytes 262176 | tf_op jit(solution)/shard_map/ppermute | solution.py:708
  53.1 1.6 %collective-permute-start.13 = (bf16[64,768]{1,0:T(8,128)(2,1)S(1)}, bf16[64,768]{1,0:T(8,128)(2,1)S(1)}, u32[]{:S(2)}, u32[]{:S(2)}) collective-permute-start(bf16[64,768]{1,0:T(8,128)(2,1)S(1)} %get-tuple-element.33), channel_id=1, source_target_pairs={{0,2},{1,3},{2,0},{3,1},{4,6},{5,7},{6,4},{7,5},{8,10},{9,11},{10,... | collective-permute-start | bytes 294920 | tf_op jit(solution)/shard_map/ppermute | solution.py:693
  54.7 1.5 %collective-permute-start.14 = (bf16[64,768]{1,0:T(8,128)(2,1)S(1)}, bf16[64,768]{1,0:T(8,128)(2,1)S(1)}, u32[]{:S(2)}, u32[]{:S(2)}) collective-permute-start(bf16[64,768]{1,0:T(8,128)(2,1)S(1)} %get-tuple-element.34), channel_id=1, source_target_pairs={{0,16},{16,0},{1,17},{17,1},{2,18},{18,2},{3,19},{19,3},{4,20},{20... | collective-permute-start | bytes 294920 | tf_op jit(solution)/shard_map/ppermute | solution.py:693
  56.9 1.6 %collective-permute-start.19 = (bf16[64,256]{1,0:T(8,128)(2,1)S(1)}, bf16[64,256]{1,0:T(8,128)(2,1)S(1)}, u32[]{:S(2)}, u32[]{:S(2)}) collective-permute-start(bf16[64,256]{1,0:T(8,128)(2,1)S(1)} %get-tuple-element.36), channel_id=1, source_target_pairs={{0,2},{1,3},{2,0},{3,1},{4,6},{5,7},{6,4},{7,5},{8,10},{9,11},{10,... | collective-permute-start | bytes 98312 | tf_op jit(solution)/shard_map/ppermute | solution.py:693
  58.5 1.5 %collective-permute-start.20 = (bf16[64,256]{1,0:T(8,128)(2,1)S(1)}, bf16[64,256]{1,0:T(8,128)(2,1)S(1)}, u32[]{:S(2)}, u32[]{:S(2)}) collective-permute-start(bf16[64,256]{1,0:T(8,128)(2,1)S(1)} %get-tuple-element.37), channel_id=1, source_target_pairs={{0,16},{16,0},{1,17},{17,1},{2,18},{18,2},{3,19},{19,3},{4,20},{20... | collective-permute-start | bytes 98312 | tf_op jit(solution)/shard_map/ppermute | solution.py:693
  60.0 1.5 %collective-permute-done.19.refs_5_ = bf16[64,256]{1,0:T(8,128)(2,1)S(1)} collective-permute-done((bf16[64,256]{1,0:T(8,128)(2,1)S(1)}, bf16[64,256]{1,0:T(8,128)(2,1)S(1)}, u32[]{:S(2)}, u32[]{:S(2)}) %collective-permute-start.19) | collective-permute-done | bytes 32800 | tf_op jit(solution)/shard_map/ppermute | solution.py:693
  61.5 2.2 %collective-permute-start.21 = (bf16[64,256]{1,0:T(8,128)(2,1)S(1)}, bf16[64,256]{1,0:T(8,128)(2,1)S(1)}, u32[]{:S(2)}, u32[]{:S(2)}) collective-permute-start(bf16[64,256]{1,0:T(8,128)(2,1)S(1)} %get-tuple-element.38), channel_id=1, source_target_pairs={{0,18},{1,19},{2,16},{3,17},{16,2},{17,3},{18,0},{19,1},{4,22},{5,... | collective-permute-start | bytes 98312 | tf_op jit(solution)/shard_map/ppermute | solution.py:749
  63.7 2.6 %collective-permute-done.21.refs_7_ = bf16[64,256]{1,0:T(8,128)(2,1)S(1)} collective-permute-done((bf16[64,256]{1,0:T(8,128)(2,1)S(1)}, bf16[64,256]{1,0:T(8,128)(2,1)S(1)}, u32[]{:S(2)}, u32[]{:S(2)}) %collective-permute-start.21) | collective-permute-done | bytes 32800 | tf_op jit(solution)/shard_map/ppermute | solution.py:749
  (37 shorter events, 8.9 us)
Async XLA Ops:
  0.0 6.2 %copy-start = (bf16[2,256,512]{2,1,0:T(8,128)(2,1)S(1)}, bf16[2,256,512]{2,1,0:T(8,128)(2,1)}, u32[]{:S(2)}) copy-start(bf16[2,256,512]{2,1,0:T(8,128)(2,1)} %param.27) | copy-start | bytes 1572868
  2.3 13.1 %collective-permute-start.1 = (bf16[400,256]{1,0:T(8,128)(2,1)S(1)}, bf16[400,256]{1,0:T(8,128)(2,1)S(1)}, u32[]{:S(2)}, u32[]{:S(2)}) collective-permute-start(bf16[400,256]{1,0:T(8,128)(2,1)S(1)} %get-tuple-element.25.own_ref), channel_id=1, source_target_pairs={{4,8},{5,9},{6,10},{7,11},{20,24},{21,25},{22,26},{23,27}} | collective-permute-start | bytes 614408 | tf_op jit(solution)/shard_map/ppermute | solution.py:699
  3.6 12.5 %collective-permute-start.2 = (bf16[400,256]{1,0:T(8,128)(2,1)S(1)}, bf16[400,256]{1,0:T(8,128)(2,1)S(1)}, u32[]{:S(2)}, u32[]{:S(2)}) collective-permute-start(bf16[400,256]{1,0:T(8,128)(2,1)S(1)} %get-tuple-element.25.own_ref), channel_id=1, source_target_pairs={{0,8},{1,9},{2,10},{3,11},{16,24},{17,25},{18,26},{19,27}} | collective-permute-start | bytes 614408 | tf_op jit(solution)/shard_map/ppermute | solution.py:700
  4.9 13.3 %collective-permute-start.4 = (bf16[512,256]{1,0:T(8,128)(2,1)S(1)}, bf16[512,256]{1,0:T(8,128)(2,1)S(1)}, u32[]{:S(2)}, u32[]{:S(2)}) collective-permute-start(bf16[512,256]{1,0:T(8,128)(2,1)S(1)} %get-tuple-element.26), channel_id=1, source_target_pairs={{12,8},{13,9},{14,10},{15,11},{28,24},{29,25},{30,26},{31,27}} | collective-permute-start | bytes 786440 | tf_op jit(solution)/shard_map/ppermute | solution.py:697
  6.2 26.1 %collective-permute-start.9 = (bf16[2,256,256]{2,1,0:T(8,128)(2,1)S(1)}, bf16[2,256,256]{2,1,0:T(8,128)(2,1)S(1)}, u32[]{:S(2)}, u32[]{:S(2)}) collective-permute-start(bf16[2,256,256]{2,1,0:T(8,128)(2,1)S(1)} %constant_dynamic-slice_fusion.refs_6_), channel_id=1, source_target_pairs={{0,4},{4,0},{8,12},{12,8},{1,5},{5,1},{9,13},{13,9},{2,6},{6,2},{1... | collective-permute-start | bytes 786440 | tf_op jit(solution)/shard_map/ppermute | solution.py:693
  8.9 24.0 %collective-permute-start.10 = (bf16[2,256,256]{2,1,0:T(8,128)(2,1)S(1)}, bf16[2,256,256]{2,1,0:T(8,128)(2,1)S(1)}, u32[]{:S(2)}, u32[]{:S(2)}) collective-permute-start(bf16[2,256,256]{2,1,0:T(8,128)(2,1)S(1)} %constant_dynamic-slice_fusion.refs_6_), channel_id=1, source_target_pairs={{0,12},{12,0},{1,13},{13,1},{2,14},{14,2},{3,15},{15,3},{16,28},{2... | collective-permute-start | bytes 786440 | tf_op jit(solution)/shard_map/ppermute | solution.py:707
  15.4 6.2 %collective-permute-start = (bf16[400,256]{1,0:T(8,128)(2,1)S(1)}, bf16[400,256]{1,0:T(8,128)(2,1)S(1)}, u32[]{:S(2)}, u32[]{:S(2)}) collective-permute-start(bf16[400,256]{1,0:T(8,128)(2,1)S(1)} %get-tuple-element.25.own_ref), channel_id=1, source_target_pairs={{0,4},{1,5},{2,6},{3,7},{16,20},{17,21},{18,22},{19,23}} | collective-permute-start | bytes 614408 | tf_op jit(solution)/shard_map/ppermute | solution.py:698
  16.1 18.4 %collective-permute-start.11 = (bf16[2,256,256]{2,1,0:T(8,128)(2,1)S(1)}, bf16[2,256,256]{2,1,0:T(8,128)(2,1)S(1)}, u32[]{:S(2)}, u32[]{:S(2)}) collective-permute-start(bf16[2,256,256]{2,1,0:T(8,128)(2,1)S(1)} %constant_dynamic-slice_fusion.refs_6_), channel_id=1, source_target_pairs={{4,8},{8,4},{5,9},{9,5},{6,10},{10,6},{7,11},{11,7},{20,24},{24,20... | collective-permute-start | bytes 786440 | tf_op jit(solution)/shard_map/ppermute | solution.py:706
  18.2 6.6 %collective-permute-start.3 = (bf16[128,256]{1,0:T(8,128)(2,1)S(1)}, bf16[128,256]{1,0:T(8,128)(2,1)S(1)}, u32[]{:S(2)}, u32[]{:S(2)}) collective-permute-start(bf16[128,256]{1,0:T(8,128)(2,1)S(1)} %blend.1), channel_id=1, source_target_pairs={{8,12},{9,13},{10,14},{11,15},{24,28},{25,29},{26,30},{27,31}} | collective-permute-start | bytes 196616 | tf_op jit(solution)/shard_map/ppermute | solution.py:710
  21.6 12.9 %collective-permute-start.7 = (bf16[256,256]{1,0:T(8,128)(2,1)S(1)}, bf16[256,256]{1,0:T(8,128)(2,1)S(1)}, u32[]{:S(2)}, u32[]{:S(2)}) collective-permute-start(bf16[256,256]{1,0:T(8,128)(2,1)S(1)} %shard_map.136), channel_id=1, source_target_pairs={{8,12},{9,13},{10,14},{11,15},{24,28},{25,29},{26,30},{27,31}} | collective-permute-start | bytes 393224 | tf_op jit(solution)/shard_map/ppermute | solution.py:713
  24.8 9.7 %collective-permute-start.8 = (bf16[256,256]{1,0:T(8,128)(2,1)S(1)}, bf16[256,256]{1,0:T(8,128)(2,1)S(1)}, u32[]{:S(2)}, u32[]{:S(2)}) collective-permute-start(bf16[256,256]{1,0:T(8,128)(2,1)S(1)} %shard_map.136), channel_id=1, source_target_pairs={{8,28},{24,12},{9,29},{25,13},{10,30},{26,14},{11,31},{27,15}} | collective-permute-start | bytes 393224 | tf_op jit(solution)/shard_map/ppermute | solution.py:726
  32.3 6.1 %collective-permute-start.5 = (bf16[256,256]{1,0:T(8,128)(2,1)S(1)}, bf16[256,256]{1,0:T(8,128)(2,1)S(1)}, u32[]{:S(2)}, u32[]{:S(2)}) collective-permute-start(bf16[256,256]{1,0:T(8,128)(2,1)S(1)} %carry.1.refs_0_), channel_id=1, source_target_pairs={{0,16},{16,0},{1,17},{17,1},{2,18},{18,2},{3,19},{19,3},{4,20},{20... | collective-permute-start | bytes 393224 | tf_op jit(solution)/shard_map/ppermute | solution.py:693
  32.9 6.9 %collective-permute-start.6 = (bf16[256,256]{1,0:T(8,128)(2,1)S(1)}, bf16[256,256]{1,0:T(8,128)(2,1)S(1)}, u32[]{:S(2)}, u32[]{:S(2)}) collective-permute-start(bf16[256,256]{1,0:T(8,128)(2,1)S(1)} %shard_map.137.refs_2_), channel_id=1, source_target_pairs={{0,16},{16,0},{1,17},{17,1},{2,18},{18,2},{3,19},{19,3},{4,20},{20... | collective-permute-start | bytes 393224 | tf_op jit(solution)/shard_map/ppermute | solution.py:693
  40.2 12.8 %collective-permute-start.12 = (bf16[256,768]{1,0:T(8,128)(2,1)S(1)}, bf16[256,768]{1,0:T(8,128)(2,1)S(1)}, u32[]{:S(2)}, u32[]{:S(2)}) collective-permute-start(bf16[256,768]{1,0:T(8,128)(2,1)S(1)} %project.5), channel_id=1, source_target_pairs={{0,1},{1,0},{2,3},{3,2},{4,5},{5,4},{6,7},{7,6},{8,9},{9,8},{10,11... | collective-permute-start | bytes 1179656 | tf_op jit(solution)/shard_map/ppermute | solution.py:693
  40.3 7.9 %collective-permute-start.16 = (bf16[2,256,256]{2,1,0:T(8,128)(2,1)S(1)}, bf16[2,256,256]{2,1,0:T(8,128)(2,1)S(1)}, u32[]{:S(2)}, u32[]{:S(2)}) collective-permute-start(bf16[2,256,256]{2,1,0:T(8,128)(2,1)S(1)} %collective-permute-done.11.refs_9_), channel_id=1, source_target_pairs={{4,0},{8,12},{5,1},{9,13},{6,2},{10,14},{7,3},{11,15},{20,16},{24,... | collective-permute-start | bytes 786440 | tf_op jit(solution)/shard_map/ppermute | solution.py:709
  42.0 10.3 %collective-permute-start.17 = (bf16[2,256,256]{2,1,0:T(8,128)(2,1)S(1)}, bf16[2,256,256]{2,1,0:T(8,128)(2,1)S(1)}, u32[]{:S(2)}, u32[]{:S(2)}) collective-permute-start(bf16[2,256,256]{2,1,0:T(8,128)(2,1)S(1)} %collective-permute-done.9.refs_7_), channel_id=1, source_target_pairs={{4,8},{8,4},{5,9},{9,5},{6,10},{10,6},{7,11},{11,7},{20,24},{24,20... | collective-permute-start | bytes 786440 | tf_op jit(solution)/shard_map/ppermute | solution.py:708
  52.6 4.3 %collective-permute-start.18 = (bf16[256,256]{1,0:T(8,128)(2,1)S(1)}, bf16[256,256]{1,0:T(8,128)(2,1)S(1)}, u32[]{:S(2)}, u32[]{:S(2)}) collective-permute-start(bf16[256,256]{1,0:T(8,128)(2,1)S(1)} %project.7), channel_id=1, source_target_pairs={{0,1},{1,0},{2,3},{3,2},{4,5},{5,4},{6,7},{7,6},{8,9},{9,8},{10,11... | collective-permute-start | bytes 393224 | tf_op jit(solution)/shard_map/ppermute | solution.py:693
  53.1 13.2 %collective-permute-start.13 = (bf16[64,768]{1,0:T(8,128)(2,1)S(1)}, bf16[64,768]{1,0:T(8,128)(2,1)S(1)}, u32[]{:S(2)}, u32[]{:S(2)}) collective-permute-start(bf16[64,768]{1,0:T(8,128)(2,1)S(1)} %get-tuple-element.33), channel_id=1, source_target_pairs={{0,2},{1,3},{2,0},{3,1},{4,6},{5,7},{6,4},{7,5},{8,10},{9,11},{10,... | collective-permute-start | bytes 294920 | tf_op jit(solution)/shard_map/ppermute | solution.py:693
  54.7 11.7 %collective-permute-start.14 = (bf16[64,768]{1,0:T(8,128)(2,1)S(1)}, bf16[64,768]{1,0:T(8,128)(2,1)S(1)}, u32[]{:S(2)}, u32[]{:S(2)}) collective-permute-start(bf16[64,768]{1,0:T(8,128)(2,1)S(1)} %get-tuple-element.34), channel_id=1, source_target_pairs={{0,16},{16,0},{1,17},{17,1},{2,18},{18,2},{3,19},{19,3},{4,20},{20... | collective-permute-start | bytes 294920 | tf_op jit(solution)/shard_map/ppermute | solution.py:693
  56.2 10.1 %collective-permute-start.15 = (bf16[64,768]{1,0:T(8,128)(2,1)S(1)}, bf16[64,768]{1,0:T(8,128)(2,1)S(1)}, u32[]{:S(2)}, u32[]{:S(2)}) collective-permute-start(bf16[64,768]{1,0:T(8,128)(2,1)S(1)} %get-tuple-element.35), channel_id=1, source_target_pairs={{0,18},{1,19},{2,16},{3,17},{16,2},{17,3},{18,0},{19,1},{4,22},{5,... | collective-permute-start | bytes 294920 | tf_op jit(solution)/shard_map/ppermute | solution.py:749
  56.9 4.6 %collective-permute-start.19 = (bf16[64,256]{1,0:T(8,128)(2,1)S(1)}, bf16[64,256]{1,0:T(8,128)(2,1)S(1)}, u32[]{:S(2)}, u32[]{:S(2)}) collective-permute-start(bf16[64,256]{1,0:T(8,128)(2,1)S(1)} %get-tuple-element.36), channel_id=1, source_target_pairs={{0,2},{1,3},{2,0},{3,1},{4,6},{5,7},{6,4},{7,5},{8,10},{9,11},{10,... | collective-permute-start | bytes 98312 | tf_op jit(solution)/shard_map/ppermute | solution.py:693
  58.5 5.2 %collective-permute-start.20 = (bf16[64,256]{1,0:T(8,128)(2,1)S(1)}, bf16[64,256]{1,0:T(8,128)(2,1)S(1)}, u32[]{:S(2)}, u32[]{:S(2)}) collective-permute-start(bf16[64,256]{1,0:T(8,128)(2,1)S(1)} %get-tuple-element.37), channel_id=1, source_target_pairs={{0,16},{16,0},{1,17},{17,1},{2,18},{18,2},{3,19},{19,3},{4,20},{20... | collective-permute-start | bytes 98312 | tf_op jit(solution)/shard_map/ppermute | solution.py:693
  61.5 4.8 %collective-permute-start.21 = (bf16[64,256]{1,0:T(8,128)(2,1)S(1)}, bf16[64,256]{1,0:T(8,128)(2,1)S(1)}, u32[]{:S(2)}, u32[]{:S(2)}) collective-permute-start(bf16[64,256]{1,0:T(8,128)(2,1)S(1)} %get-tuple-element.38), channel_id=1, source_target_pairs={{0,18},{1,19},{2,16},{3,17},{16,2},{17,3},{18,0},{19,1},{4,22},{5,... | collective-permute-start | bytes 98312 | tf_op jit(solution)/shard_map/ppermute | solution.py:749
